TPU v7x, 256 devices: a whole 4x4x8 slice. The times are simulated.
256 devices in a mesh: rep: 2 (over z_hi), fs: 16 (over z_lo, x), tp: 8 (over y, core).
Axes of the slice: x: 4, y: 4, z: 8 (z_hi: 2, z_lo: 4; z = z_hi * 4 + z_lo), core: 2. Of those that a mesh axis runs over, the one named last changes fastest.
Arguments:
- stream: bfloat16 [32768, 2048], P(('rep', 'fs', 'tp')), may hold values from -6 to 6
- gate_weight: bfloat16 [2048, 2816], P('fs', 'tp'), may hold values from -0.125 to 0.125
- up_weight: bfloat16 [2048, 2816], P('fs', 'tp'), may hold values from -0.125 to 0.125
- down_weight: bfloat16 [2816, 2048], P('tp', 'fs'), may hold values from -0.21875 to 0.21875
- query_weight: bfloat16 [2048, 512], P('fs', 'tp'), may hold values from -0.125 to 0.125
- key_weight: bfloat16 [2048, 512], P('fs', 'tp'), may hold values from -0.125 to 0.125
- value_weight: bfloat16 [2048, 1024], P('fs', 'tp'), may hold values from -0.125 to 0.125
- outgate_weight: bfloat16 [2048, 1024], P('fs', 'tp'), may hold values from -0.125 to 0.125
- decay_down: bfloat16 [2048, 32], replicated, may hold values from -0.125 to 0.125
- decay_up: bfloat16 [32, 512], P(None, 'tp'), may hold values from -2 to 2
- decay_bias: float32 [512], P('tp'), may hold values from -0.5 to 7
- head_gain: float32 [128], replicated, may hold values from 0.1 to 1.9
- out_weight: bfloat16 [1024, 2048], P('tp', 'fs'), may hold values from -0.375 to 0.375
- norm_gain: float32 [3, 2048], replicated, may hold values from 0.1 to 1.9
Outputs:
- layer_out: bfloat16 [32768, 2048], P(('rep', 'fs', 'tp'))
All inputs are finite; a program needn't handle non-finite values.
Results may differ from a plain program's by a relative error of at most 0.015.
Values may be sent and summed in bfloat16 or wider, within the bound.
A program may use at most 128 MiB of HBM per device.

v0:
```python
import jax
import jax.numpy as jnp
from jax import lax
from jax.sharding import PartitionSpec as P

DK = 64
DV = 128
BLOCK = 64


RESIDUAL_SCALE = 2.0**0.5
BRANCH_SCALE = 0.5
NORM_EPS = 1e-05
HEAD_EPS = 0.01
GATE_DIVISOR = 16.0


def from_everyone(value, axis):
    copies = jnp.broadcast_to(value, (lax.axis_size(axis), *value.shape))
    return lax.all_to_all(copies, axis, split_axis=0, concat_axis=0, tiled=True)


def joined_along(pieces, dim):
    pieces = jnp.moveaxis(pieces, 0, dim)
    lengths = pieces.shape
    return pieces.reshape(*lengths[:dim], lengths[dim] * lengths[dim + 1], *lengths[dim + 2 :])


def gather_directly(value, axis, dim):
    pieces = from_everyone(value, axis)
    return joined_along(pieces, dim)


def side_by_side(arrays, axis, dim, along):
    widths = [a.shape[along] for a in arrays]
    both = jnp.concatenate(arrays, axis=along)
    result = lax.all_gather(both, axis, axis=dim, tiled=True)
    return tuple(jnp.split(result, [sum(widths[:k]) for k in range(1, len(widths))], axis=along))


def layer_norm(values, norm_scale):
    average = jnp.mean(values, -1, keepdims=True)
    centred = values - average
    spread = jnp.mean(centred * centred, -1, keepdims=True)
    return (centred * lax.rsqrt(spread + NORM_EPS) * norm_scale).astype(jnp.bfloat16)


def blocked_mixer(query, key_rows, value_rows, log_gate):
    length, head_count, key_dim = query.shape
    value_dim = value_rows.shape[2]
    block_count = length // BLOCK

    def split_blocks(values):
        return values.reshape(block_count, BLOCK, head_count, values.shape[2]).transpose(0, 2, 1, 3)

    causal = jnp.tril(jnp.ones((BLOCK, BLOCK), dtype=bool))

    def advance(carried, inputs):
        query_blk, key_blk, value_blk, decay_blk = inputs
        log_gaps = decay_blk[:, :, None, :] - decay_blk[:, None, :, :]
        log_gaps = jnp.where(causal[None, :, :, None], log_gaps, -jnp.inf)
        scores = jnp.sum(
            query_blk[:, :, None, :] * key_blk[:, None, :, :] * jnp.exp(log_gaps), axis=-1
        )
        inside = jnp.einsum("hij,hjv->hiv", scores, value_blk)
        carried_part = jnp.einsum("hid,hdv->hiv", query_blk * jnp.exp(decay_blk), carried)
        closing = decay_blk[:, -1, :]
        update = jnp.einsum(
            "hjd,hjv->hdv", key_blk * jnp.exp(closing[:, None, :] - decay_blk), value_blk
        )
        return (carried * jnp.exp(closing)[:, :, None] + update, inside + carried_part)

    cumulative = jnp.cumsum(split_blocks(log_gate), axis=2)
    start_state = jnp.zeros((head_count, key_dim, value_dim), jnp.float32)
    _, outputs = lax.scan(
        advance,
        start_state,
        (split_blocks(query), split_blocks(key_rows), split_blocks(value_rows), cumulative),
    )
    return outputs.transpose(0, 2, 1, 3).reshape(length, head_count, value_dim)


def on_device(
    stream,
    gate_weight,
    up_weight,
    down_weight,
    query_weight,
    key_weight,
    value_weight,
    outgate_weight,
    decay_down,
    decay_up,
    decay_bias,
    head_gain,
    out_weight,
    norm_gain,
):
    down_local = gather_directly(down_weight, "fs", 1)
    down_full = lax.all_gather(down_local, "tp", axis=0, tiled=True)

    def ffn_half(current, norm_scale):
        gathered = lax.all_gather(current, "tp", axis=0, tiled=True)
        pieces = side_by_side((gate_weight, up_weight), "fs", 0, 1)
        gate = jnp.dot(gathered, pieces[0], preferred_element_type=jnp.float32)
        upward = jnp.dot(gathered, pieces[1], preferred_element_type=jnp.float32)
        hidden = (jax.nn.silu(gate) * upward).astype(jnp.bfloat16)
        own_hidden = lax.all_to_all(hidden, "tp", split_axis=0, concat_axis=1, tiled=True)
        summed = jnp.dot(own_hidden, down_full, preferred_element_type=jnp.float32)
        return layer_norm(
            RESIDUAL_SCALE * current.astype(jnp.float32) + BRANCH_SCALE * summed, norm_scale
        )

    first = ffn_half(stream, norm_gain[0])
    gathered = lax.all_gather(first, "tp", axis=0, tiled=True)
    length = gathered.shape[0]
    pieces = side_by_side((query_weight, key_weight, value_weight, outgate_weight), "fs", 0, 1)
    query, key_rows, value_rows, outgate = tuple(
        (jnp.dot(gathered, piece, preferred_element_type=jnp.float32) for piece in pieces)
    )
    query = query.astype(jnp.bfloat16)
    key_rows = key_rows.astype(jnp.bfloat16)
    value_rows = value_rows.astype(jnp.bfloat16)
    outgate = outgate.astype(jnp.bfloat16)
    low_rank = jnp.dot(gathered, decay_down, preferred_element_type=jnp.float32).astype(
        jnp.bfloat16
    )
    pre_gate = jnp.dot(low_rank, decay_up, preferred_element_type=jnp.float32) + decay_bias
    log_gate = jax.nn.log_sigmoid(pre_gate) / GATE_DIVISOR
    local_heads = query.shape[1] // DK
    mixed = blocked_mixer(
        query.astype(jnp.float32).reshape(length, local_heads, DK) * DK ** (-0.5),
        key_rows.astype(jnp.float32).reshape(length, local_heads, DK),
        value_rows.astype(jnp.float32).reshape(length, local_heads, DV),
        log_gate.reshape(length, local_heads, DK),
    )
    normed = mixed * lax.rsqrt(jnp.mean(mixed * mixed, -1, keepdims=True) + HEAD_EPS) * head_gain
    gated = (
        normed.reshape(length, local_heads * DV) * jax.nn.silu(outgate.astype(jnp.float32))
    ).astype(jnp.bfloat16)
    out_local = gather_directly(out_weight, "fs", 1)
    out_full = lax.all_gather(out_local, "tp", axis=0, tiled=True)
    own_gated = lax.all_to_all(gated, "tp", split_axis=0, concat_axis=1, tiled=True)
    summed = jnp.dot(own_gated, out_full, preferred_element_type=jnp.float32)
    second = layer_norm(RESIDUAL_SCALE * first.astype(jnp.float32) + summed, norm_gain[1])
    return ffn_half(second, norm_gain[2])


def solution(mesh):
    in_specs = (
        P(("rep", "fs", "tp"), None),
        P("fs", "tp"),
        P("fs", "tp"),
        P("tp", "fs"),
        P("fs", "tp"),
        P("fs", "tp"),
        P("fs", "tp"),
        P("fs", "tp"),
        P(),
        P(None, "tp"),
        P("tp"),
        P(),
        P("tp", "fs"),
        P(),
    )
    out_specs = P(("rep", "fs", "tp"), None)
    return jax.shard_map(
        on_device, mesh=mesh, in_specs=in_specs, out_specs=out_specs, check_vma=False
    )
```

profile of v0, /device:TPU:1, one launch (start us, length us, event | category | flops | bytes accessed | tf_op | source)
XLA Modules:
  0.0 473.2 jit_solution(7399616951409170826)
XLA Ops:
  6.5 1.7 pad_maximum_fusion
  9.0 1.1 broadcast_in_dim.32
  10.1 57.1 %all_to_all.67 = bf16[16,352,128]{2,1,0:T(8,128)(2,1)S(1)} all-to-all(bf16[16,352,128]{2,1,0:T(8,128)(2,1)S(1)} %broadcast_in_dim.32), channel_id=1, replica_groups=mesh['rep'=2,'fs'=16,'tp'=8] {'fs'}, dimensions={0} | all-to-all | bytes 2883584 | tf_op jit(solution)/shard_map/all_to_all | solution.py:20
  67.2 1.3 copy_bitcast_fusion
  69.6 27.4 %all-gather.8.cloned.1.call-done = bf16[2048,704]{0,1:T(8,128)(2,1)} async-done(((bf16[128,704]{0,1:T(8,128)(2,1)}), bf16[2048,704]{0,1:T(8,128)(2,1)}) %all-gather.8.cloned.1.call-update) | async-done | bytes 2883600 | tf_op jit(solution)/shard_map/all_gather | solution.py:37
  97.0 44.9 %all-gather.10.cloned.1.call-done = bf16[1024,2048]{1,0:T(8,128)(2,1)} async-done(((bf16[128,2048]{1,0:T(8,128)(2,1)}), bf16[1024,2048]{1,0:T(8,128)(2,1)}) %all-gather.10.cloned.1.call-update) | async-done | bytes 4194320 | tf_op jit(solution)/shard_map/all_gather | solution.py:103
  141.9 4.5 convolution_bitcast_fusion.2
  146.4 1.9 fusion.35
  149.3 3.7 all-to-all-start
  153.1 14.9 %all-to-all-done = bf16[8,128,352]{1,2,0:T(8,128)(2,1)S(1)} async-done(((bf16[8,128,352]{1,2,0:T(8,128)(2,1)}), bf16[8,128,352]{1,2,0:T(8,128)(2,1)S(1)}, u32[]{:S(2)}, u32[]{:S(2)}) %all-to-all-start) | async-done | bytes 720928 | tf_op jit(solution)/shard_map/all_to_all | solution.py:108
  168.0 45.3 %all-gather.12.cloned.1.call-done = bf16[2816,2048]{1,0:T(8,128)(2,1)} async-done(((bf16[352,2048]{1,0:T(8,128)(2,1)}), bf16[2816,2048]{1,0:T(8,128)(2,1)}) %all-gather.12.cloned.1.call-update) | async-done | bytes 11534352 | tf_op jit(solution)/shard_map/all_gather | solution.py:100
  213.3 6.0 %fusion.58 = (f32[128]{0:T(128)S(1)}, f32[128,2048]{1,0:T(8,128)S(1)}) fusion(bf16[128,2816]{0,1:T(8,128)(2,1)S(1)} %bitcast.148, bf16[2816,2048]{1,0:T(8,128)(2,1)} %all-gather.12.cloned.1.call-done, bf16[128,2048]{1,0:T(8,128)(2,1)S(1)} %copy-done.3), kind=kOutput, calls=%fused_computation.96 | convolution fusion | flops 1477705600 | bytes 13828608 | tf_op jit(solution)/shard_map/dot_general | solution.py:109
  221.7 7.0 %all-to-all-start.3 = ((bf16[16,128,128]{1,2,0:T(8,128)(2,1)}), bf16[16,128,128]{1,2,0:T(8,128)(2,1)S(1)}, u32[]{:S(2)}, u32[]{:S(2)}) async-start(bf16[16,128,128]{1,2,0:T(8,128)(2,1)} %broadcast_in_dim.35), calls=%async_computation.3 | async-start | bytes 1048576 | tf_op jit(solution)/shard_map/all_to_all | solution.py:20
  229.0 17.3 %all-to-all-done.3 = bf16[16,128,128]{1,2,0:T(8,128)(2,1)S(1)} async-done(((bf16[16,128,128]{1,2,0:T(8,128)(2,1)}), bf16[16,128,128]{1,2,0:T(8,128)(2,1)S(1)}, u32[]{:S(2)}, u32[]{:S(2)}) %all-to-all-start.3) | async-done | bytes 524320 | tf_op jit(solution)/shard_map/all_to_all | solution.py:20
  247.2 39.2 %all-gather.16.cloned.1.call-done = bf16[2048,384]{1,0:T(8,128)(2,1)} async-done(((bf16[128,384]{1,0:T(8,128)(2,1)}), bf16[2048,384]{1,0:T(8,128)(2,1)}) %all-gather.16.cloned.1.call-update) | async-done | bytes 1572880 | tf_op jit(solution)/shard_map/all_gather | solution.py:37
  286.4 45.3 %all-gather.14.cloned.1.call-done = bf16[1024,2048]{1,0:T(8,128)(2,1)} async-done(((bf16[128,2048]{1,0:T(8,128)(2,1)}), bf16[1024,2048]{1,0:T(8,128)(2,1)}) %all-gather.14.cloned.1.call-update) | async-done | bytes 4194320 | tf_op jit(solution)/shard_map/all_gather | solution.py:115
  331.8 3.8 fusion.45
  335.7 3.7 fusion.44
  339.7 3.8 fusion.56
  344.0 6.3 %fusion.61 = f32[16,1,64,64]{3,0,1,2:T(8,128)S(1)} fusion(f32[16,1,64,64]{3,0,1,2:T(8,128)S(1)} %copy.47), kind=kOutput, calls=%fused_computation.99 | output fusion | flops 4128768 | bytes 524288 | tf_op jit(solution)/shard_map/jit(cumsum)/reduce_window_sum | solution.py:73
  350.3 3.6 convolution_convert_fusion.1
  353.9 30.5 %while.13 = (s32[]{:T(128)}, f32[1,64,128]{2,1,0:T(8,128)S(1)}, f32[16,1,64,128]{3,2,1,0:T(8,128)S(1)}, f32[16,1,64,64]{3,0,1,2:T(8,128)S(1)}, f32[16,1,64,64]{3...) while((s32[]{:T(128)}, f32[1,64,128]{2,1,0:T(8,128)S(1)}, ...), condition=%wide.region_5.6_spmd.clone, body=%wide.region_3.5_spmd.clone.sunk | while | flops 4509699 | bytes 544884 | solution.py:75
  354.0 1.4 multiply_reduce_fusion.6
  355.9 1.4 multiply_reduce_fusion.6
  357.8 1.4 multiply_reduce_fusion.6
  359.7 1.4 multiply_reduce_fusion.6
  361.6 1.4 multiply_reduce_fusion.6
  363.5 1.4 multiply_reduce_fusion.6
  365.4 1.4 multiply_reduce_fusion.6
  367.3 1.4 multiply_reduce_fusion.6
  369.2 1.4 multiply_reduce_fusion.6
  371.1 1.4 multiply_reduce_fusion.6
  373.0 1.4 multiply_reduce_fusion.6
  374.9 1.4 multiply_reduce_fusion.6
  376.8 1.4 multiply_reduce_fusion.6
  378.7 1.4 multiply_reduce_fusion.6
  380.6 1.4 multiply_reduce_fusion.6
  382.6 1.4 multiply_reduce_fusion.6
  384.7 3.6 fusion.52
  389.2 3.6 all-to-all-start.2
  392.8 6.5 %all-to-all-done.2 = bf16[8,128,128]{1,2,0:T(8,128)(2,1)S(1)} async-done(((bf16[8,128,128]{1,2,0:T(8,128)(2,1)}), bf16[8,128,128]{1,2,0:T(8,128)(2,1)S(1)}, u32[]{:S(2)}, u32[]{:S(2)}) %all-to-all-start.2) | async-done | bytes 262176 | tf_op jit(solution)/shard_map/all_to_all | solution.py:143
  399.3 3.8 fusion.59
  403.3 1.0 multiply_convert_fusion.1
  404.4 35.0 %all-gather.20.cloned.1.call-done = bf16[1024,2048]{1,0:T(8,128)(2,1)} async-done(((bf16[128,2048]{1,0:T(8,128)(2,1)}), bf16[1024,2048]{1,0:T(8,128)(2,1)}) %all-gather.20.cloned.1.call-update) | async-done | bytes 4194320 | tf_op jit(solution)/shard_map/all_gather | solution.py:103
  439.3 4.5 fusion.38
  443.8 4.6 fusion.34
  448.6 14.7 %all_to_all.68 = bf16[8,128,352]{1,2,0:T(8,128)(2,1)S(1)} all-to-all(bf16[8,128,352]{1,2,0:T(8,128)(2,1)S(1)} %bitcast.150), channel_id=1, replica_groups=mesh['rep'=2,'fs'=16,'tp'=8] {'tp'}, dimensions={0} | all-to-all | bytes 1441792 | tf_op jit(solution)/shard_map/all_to_all | solution.py:108
  463.3 1.8 fusion.60
  (211 shorter events, 18.3 us)
Async XLA Ops:
  6.5 333.1 %copy-start = (bf16[2048,32]{0,1:T(8,128)(2,1)S(1)}, bf16[2048,32]{0,1:T(8,128)(2,1)}, u32[]{:S(2)}) copy-start(bf16[2048,32]{0,1:T(8,128)(2,1)} %param.24) | copy-start | bytes 393220
  6.5 90.5 %all-gather.8.cloned.1.call-start = ((), (), s32[]{:S(2)}) async-start(), calls=%async_computation.5 | async-start | bytes 3063808 | tf_op jit(solution)/shard_map/all_gather | solution.py:37
  8.2 133.7 %all-gather.10.cloned.1.call-start = ((), (), s32[]{:S(2)}) async-start(), calls=%async_computation.6 | async-start | bytes 4718592 | tf_op jit(solution)/shard_map/all_gather | solution.py:103
  9.0 204.3 %all-gather.12.cloned.1.call-start = ((), (), s32[]{:S(2)}) async-start(), calls=%async_computation.7 | async-start | bytes 12976128 | tf_op jit(solution)/shard_map/all_gather | solution.py:100
  67.2 1.4 copy-start.9
  67.2 1.5 copy-start.10
  67.2 1.6 copy-start.5
  67.2 1.6 copy-start.6
  68.6 217.8 %all-gather.16.cloned.1.call-start = ((), (), s32[]{:S(2)}) async-start(), calls=%async_computation.9 | async-start | bytes 1671168 | tf_op jit(solution)/shard_map/all_gather | solution.py:37
  97.0 49.4 %copy-start.14 = (bf16[2048,704]{0,1:T(8,128)(2,1)S(1)}, bf16[2048,704]{0,1:T(8,128)(2,1)}, u32[]{:S(2)}) copy-start(bf16[2048,704]{0,1:T(8,128)(2,1)} %all-gather.8.cloned.1.call-done) | copy-start | bytes 8650756
  141.9 4.5 copy-start.13
  148.3 4.8 %copy-start.8 = (f32[3,2048]{1,0:T(4,128)S(1)}, f32[3,2048]{1,0:T(4,128)}, u32[]{:S(2)}) copy-start(f32[3,2048]{1,0:T(4,128)} %param.29) | copy-start | bytes 73732
  148.3 64.9 %copy-start.3 = (bf16[128,2048]{1,0:T(8,128)(2,1)S(1)}, bf16[128,2048]{1,0:T(8,128)(2,1)}, u32[]{:S(2)}) copy-start(bf16[128,2048]{1,0:T(8,128)(2,1)} %param.16) | copy-start | bytes 1572868
  149.3 18.6 %all-to-all-start = ((bf16[8,128,352]{1,2,0:T(8,128)(2,1)}), bf16[8,128,352]{1,2,0:T(8,128)(2,1)S(1)}, u32[]{:S(2)}, u32[]{:S(2)}) async-start(bf16[8,128,352]{1,2,0:T(8,128)(2,1)} %bitcast.112), calls=%async_computation | async-start | bytes 1441792 | tf_op jit(solution)/shard_map/all_to_all | solution.py:108
  153.1 178.7 %all-gather.14.cloned.1.call-start = ((), (), s32[]{:S(2)}) async-start(), calls=%async_computation.8 | async-start | bytes 4718592 | tf_op jit(solution)/shard_map/all_gather | solution.py:115
  219.3 1.3 copy-start.7
  221.7 24.6 %all-to-all-start.3 = ((bf16[16,128,128]{1,2,0:T(8,128)(2,1)}), bf16[16,128,128]{1,2,0:T(8,128)(2,1)S(1)}, u32[]{:S(2)}, u32[]{:S(2)}) async-start(bf16[16,128,128]{1,2,0:T(8,128)(2,1)} %broadcast_in_dim.35), calls=%async_computation.3 | async-start | bytes 1048576 | tf_op jit(solution)/shard_map/all_to_all | solution.py:20
  228.8 164.0 %all-gather.18.cloned.1.call-start = ((), (), s32[]{:S(2)}) async-start(), calls=%async_computation.10 | async-start | bytes 4718592 | tf_op jit(solution)/shard_map/all_gather | solution.py:142
  246.3 0.9 copy-start.4
  335.7 4.0 copy-start.11
  335.7 4.0 copy-start.12
  353.9 30.8 %copy-start.15 = (f32[128]{0:T(128)S(1)}, f32[128]{0:T(128)}, u32[]{:S(2)}) copy-start(f32[128]{0:T(128)} %param.27) | copy-start | bytes 1540
  384.7 14.6 %copy-start.1 = (bf16[128,2048]{1,0:T(8,128)(2,1)S(1)}, bf16[128,2048]{1,0:T(8,128)(2,1)}, u32[]{:S(2)}) copy-start(bf16[128,2048]{1,0:T(8,128)(2,1)} %multiply_convert_fusion.2) | copy-start | bytes 1572868
  389.2 10.1 %all-to-all-start.2 = ((bf16[8,128,128]{1,2,0:T(8,128)(2,1)}), bf16[8,128,128]{1,2,0:T(8,128)(2,1)S(1)}, u32[]{:S(2)}, u32[]{:S(2)}) async-start(bf16[8,128,128]{1,2,0:T(8,128)(2,1)} %copy.54), calls=%async_computation.2 | async-start | bytes 524288 | tf_op jit(solution)/shard_map/all_to_all | solution.py:143
  392.8 46.6 %all-gather.20.cloned.1.call-start = ((), (), s32[]{:S(2)}) async-start(), calls=%async_computation.11 | async-start | bytes 4718592 | tf_op jit(solution)/shard_map/all_gather | solution.py:103
  439.3 23.9 %slice-start = ((s8[11534336]{0:T(1024)(128)(4,1)}), s8[4194304]{0:T(1024)(128)(4,1)S(1)}, s32[]{:S(2)}) async-start(s8[11534336]{0:T(1024)(128)(4,1)} %bitcast.141), calls=%async_computation.12 | async-start | bytes 8388608
  439.3 23.9 %slice-start.1 = ((s8[11534336]{0:T(1024)(128)(4,1)}), s8[4194304]{0:T(1024)(128)(4,1)S(1)}, s32[]{:S(2)}) async-start(s8[11534336]{0:T(1024)(128)(4,1)} %bitcast.141), calls=%async_computation.13 | async-start | bytes 8388608
  443.8 19.5 %slice-start.2 = ((s8[11534336]{0:T(1024)(128)(4,1)}), s8[3145728]{0:T(1024)(128)(4,1)S(1)}, s32[]{:S(2)}) async-start(s8[11534336]{0:T(1024)(128)(4,1)} %bitcast.141), calls=%async_computation.14 | async-start | bytes 6291456
  448.4 14.8 %copy-start.2 = (bf16[128,2048]{1,0:T(8,128)(2,1)S(1)}, bf16[128,2048]{1,0:T(8,128)(2,1)}, u32[]{:S(2)}) copy-start(bf16[128,2048]{1,0:T(8,128)(2,1)} %multiply_convert_fusion.1) | copy-start | bytes 1572868
Sparse Core Ops, SparseCore 0:
  9.0 87.9 all-gather.7
  98.9 42.9 all-gather.9
  143.8 69.4 all-gather.11
  214.9 71.4 all-gather.15
  288.1 43.5 all-gather.13
  333.4 38.1 all-gather.17
  404.5 34.8 all-gather.19
where the time goes:
time: 474 us; the launch traced here: 473 us
  waiting for transfers between devices  277 us (58%)
  blocking collectives  71.8 us (15%)
  matrix products  52.6 us (11%)
  other arithmetic  34.7 us (7%)
  starting transfers between devices  14.7 us (3%)
  between operations  13.8 us (3%)
  local copies, waits for them, and re-layouts  8.37 us (2%)
    all_gather x2, waiting for transfers between devices, ffn_half(): gathered = lax.all_gather(current, 'tp', axis=0, tiled=True)  79.9 us
    all_gather x2, waiting for transfers between devices, side_by_side(): result = lax.all_gather(both, axis, axis=dim, tiled=True)  66.6 us
    all_to_all x1, blocking collectives, from_everyone(): return lax.all_to_all(copies, axis, split_axis=0, concat_axis=0, tiled=True)  57.1 us
    all_gather x1, waiting for transfers between devices, on_device(): gathered = lax.all_gather(first, 'tp', axis=0, tiled=True)  45.3 us
    all_gather x1, waiting for transfers between devices, on_device(): down_full = lax.all_gather(down_local, 'tp', axis=0, tiled=True)  45.3 us
    reduce_sum x16, other arithmetic, advance(): jnp.sum(query_blk[:, :, None, :] * key_blk[:, None, :, :] * jnp.exp(log_g...  21.7 us
    all_to_all x1, waiting for transfers between devices, from_everyone(): return lax.all_to_all(copies, axis, split_axis=0, concat_axis=0, tiled=True)  17.3 us
    all_to_all x1, waiting for transfers between devices, ffn_half(): lax.all_to_all(hidden, 'tp', split_axis=0, concat_axis=1, tiled=True)  14.9 us
  transfers between devices with their start and end apart: 10, of which 9 were waited for; matrix products, arithmetic and copies ran while one was open for 16% of the time, Pallas kernels for 0%

commit v1 on v0

v1 whole, which is shorter than its diff:
```python
import functools

import jax
import jax.numpy as jnp
from jax import lax
from jax.experimental import pallas as pl
from jax.experimental.pallas import tpu as pltpu
from jax.sharding import PartitionSpec as P

MESH = pl.DeviceIdType.MESH
F32, BF16 = jnp.float32, jnp.bfloat16
D, DK, DV, GR = 2048, 64, 128, 32
ROWS = 128
HID = 352
CHUNKS = ((0, 96, 192), (192, 272, 352))
PROJ = 384
BLK = 128
RESIDUAL_SCALE = 2.0**0.5
BRANCH_SCALE = 0.5
NORM_EPS = 1e-05
HEAD_EPS = 0.01
GATE_DIVISOR = 16.0

NT = (((1,), (1,)), ((), ()))
NN = (((1,), (0,)), ((), ()))
TN = (((0,), (0,)), ((), ()))


def dot(a, b, dims=NN, **kw):
    return lax.dot_general(a, b, dims, preferred_element_type=F32, **kw)


def place():
    r, f, t = lax.axis_index("rep"), lax.axis_index("fs"), lax.axis_index("tp")
    return r, f // 4, f % 4, t // 2, t % 2


def neighbour(dim, step):
    r, zl, x, y, c = place()
    if dim == "x":
        return (r, zl * 4 + (x + step + 4) % 4, y * 2 + c)
    if dim == "y":
        return (r, zl * 4 + x, ((y + step + 4) % 4) * 2 + c)
    if dim == "c":
        return (r, zl * 4 + x, y * 2 + 1 - c)
    z = (r * 4 + zl + step + 8) % 8
    return (z // 4, (z % 4) * 4 + x, y * 2 + c)


class Gather:
    def __init__(self, order, at, rows, send, recv, pending):
        self.order, self.at, self.rows = order, at, rows
        self.send, self.recv, self.pending = send, recv, pending
        r, zl, x, y, c = place()
        self.pos = {"x": x, "y": y, "z": zl}

    def region(self, phase, shift, lo, hi):
        idx = {}
        for k, dim in enumerate(self.order):
            if k < phase:
                idx[dim] = slice(None)
            elif k == phase:
                idx[dim] = (self.pos[dim] + shift) % 4
            else:
                idx[dim] = self.pos[dim]
        return self.at(idx, pl.ds(lo, hi - lo))

    def copy(self, phase, shift, part, stage, way):
        lo, mid, hi = self.rows
        lo, hi = ((lo, hi), (lo, mid), (mid, hi))[part]
        region = self.region(phase, shift, lo, hi)
        return pltpu.make_async_remote_copy(
            src_ref=region,
            dst_ref=region,
            send_sem=self.send(phase, stage, way),
            recv_sem=self.recv(phase, stage, way),
            device_id=neighbour(self.order[phase], 1 if way == 0 else -1),
            device_id_type=MESH,
        )

    def begin(self, phase):
        for way in (0, 1):
            cp = self.copy(phase, 0, 0, 0, way)
            cp.start()
            self.pending.append(cp)

    def pass_on(self, phase):
        for way in (0, 1):
            self.copy(phase, 3 if way == 0 else 1, 0, 0, way).wait_recv()
        for way in (0, 1):
            cp = self.copy(phase, 3 if way == 0 else 1, way + 1, 1, way)
            cp.start()
            self.pending.append(cp)

    def finish(self, phase):
        for way in (0, 1):
            self.copy(phase, 2, way + 1, 1, way).wait_recv()


def layer_norm(values, norm_scale):
    average = jnp.mean(values, -1, keepdims=True)
    centred = values - average
    spread = jnp.mean(centred * centred, -1, keepdims=True)
    return (centred * lax.rsqrt(spread + NORM_EPS) * norm_scale).astype(BF16)


def silu(v):
    return v / (1.0 + jnp.exp(-v))


def kernel(
    stop,
    x_ref, g_ref, u_ref, d_ref, q_ref, k_ref, v_ref, og_ref, dd_ref, du_ref, bias_ref, gain_ref, wo_ref, norm_ref,
    out_ref,
    W, Wa, Wo, WaW, xa, xb, hidT, hid, acc, part, fa, proj, gout, gin,
    lsem, fsend, frecv, asend, arecv, osend, orecv, csend, crecv, ysend, yrecv,
):
    r, zl, x, y, c = place()
    t = y * 2 + c
    barrier = pltpu.get_barrier_semaphore()
    for dim in "xyz":
        for step in (1, -1):
            pl.semaphore_signal(barrier, 1, device_id=neighbour(dim, step), device_id_type=MESH)
    pl.semaphore_signal(barrier, 1, device_id=neighbour("c", 1), device_id_type=MESH)
    pl.semaphore_signal(barrier, 1, device_id=neighbour("y", 2), device_id_type=MESH)
    own = []
    for w, ref in enumerate((g_ref, u_ref, d_ref)):
        own.append(pltpu.make_async_copy(ref, W.at[w, y, zl, x], lsem.at[w]))
    own.append(pltpu.make_async_copy(wo_ref, Wo.at[y, zl, x], lsem.at[3]))
    own.append(pltpu.make_async_copy(x_ref, xa.at[c], lsem.at[4]))
    for cp in own:
        cp.start()
    pl.semaphore_wait(barrier, 8)
    for cp in own:
        cp.wait()

    pending = []

    def across(src, dst, slot):
        return pltpu.make_async_remote_copy(
            src_ref=src, dst_ref=dst, send_sem=csend.at[slot], recv_sem=crecv.at[slot],
            device_id=neighbour("c", 1), device_id_type=MESH,
        )

    def swap(src, dst, slot):
        cp = across(src, dst, slot)
        cp.start()
        pending.append(cp)

    orders = (("x", "z", "y"), ("z", "y", "x"), ("y", "x", "z"))

    def ffn_gather(ch, w):
        return Gather(
            orders[w],
            lambda idx, rows: W.at[w, idx["y"], idx["z"], idx["x"], rows],
            CHUNKS[ch],
            lambda ph, st, way: fsend.at[ch, w, ph, st, way],
            lambda ph, st, way: frecv.at[ch, w, ph, st, way],
            pending,
        )

    ffn = [[ffn_gather(ch, w) for w in range(3)] for ch in range(2)]

    for w in range(3):
        ffn[0][w].begin(0)
    swap(xa.at[c], xa.at[c], 0)
    for w in range(3):
        ffn[1][w].begin(0)
    Wa[zl, x, 0:64, :] = q_ref[...]
    Wa[zl, x, 64:128, :] = k_ref[...]
    Wa[zl, x, 128:256, :] = v_ref[...].astype(F32).T.astype(BF16)
    Wa[zl, x, 256:384, :] = og_ref[...].astype(F32).T.astype(BF16)

    for ph in range(3):
        if ph:
            for ch in range(2):
                for w in range(3):
                    ffn[ch][w].finish(ph - 1)
                    ffn[ch][w].begin(ph)
        for ch in range(2):
            for w in range(3):
                ffn[ch][w].pass_on(ph)

    def hidden(ch, rows):
        lo, _, hi = CHUNKS[ch]
        size = hi - lo

        def body(yy, _):
            both = rows[...].reshape(2 * ROWS, D)
            gate, up = (
                dot(
                    jnp.concatenate(
                        [W[w, yy, f // 4, f % 4, lo:hi, :] for f in range(16)], axis=1
                    ),
                    both,
                    NT,
                )
                for w in (0, 1)
            )
            hidT[pl.ds(pl.multiple_of(yy * size, 16), size), :] = silu(gate) * up
            return 0

        lax.fori_loop(0, 4, body, 0)
        hid[:, : 4 * size] = hidT[: 4 * size, :].T.astype(BF16)

    def down(ch):
        lo, _, hi = CHUNKS[ch]
        size = hi - lo

        def body(j, _):
            weights = jnp.concatenate(
                [
                    jnp.concatenate([W[2, yy, j // 2, (j % 2) * 2 + i, lo:hi, :] for i in range(2)], axis=1)
                    for yy in range(4)
                ],
                axis=0,
            )
            cols = pl.ds(pl.multiple_of(j * 256, 256), 256)
            term = dot(hid[:, : 4 * size], weights)
            for half in range(2):
                piece = term[half * ROWS : (half + 1) * ROWS]
                if ch:
                    acc[half, :, cols] += piece
                else:
                    acc[half, :, cols] = piece
            return 0

        lax.fori_loop(0, 8, body, 0)

    def joined(slot, residual, scale, branch, norm):
        across(acc.at[c], part.at[slot], 2 + slot).wait_recv()
        total = acc[c] + part[slot]
        return layer_norm(scale * residual.astype(F32) + branch * total, norm_ref[norm : norm + 1, :])

    for ch in range(2):
        if ch == 0:
            across(xa.at[c], xa.at[c], 0).wait_recv()
        for w in range(3):
            ffn[ch][w].finish(2)
        hidden(ch, xa)
        down(ch)
    swap(acc.at[1 - c], part.at[0], 2)
    first = joined(0, xa[c], RESIDUAL_SCALE, BRANCH_SCALE, 0)
    fa[t] = first
    if stop == 1:
        out_ref[...] = fa[t]

    if stop != 1:
        def along(block, rows, slot, step):
            ref = fa.at[block, rows]
            return pltpu.make_async_remote_copy(
                src_ref=ref, dst_ref=ref, send_sem=ysend.at[slot], recv_sem=yrecv.at[slot],
                device_id=neighbour("y", step), device_id_type=MESH,
            )

        def go(cp):
            cp.start()
            pending.append(cp)

        every, low_half, high_half = pl.ds(0, ROWS), pl.ds(0, ROWS // 2), pl.ds(ROWS // 2, ROWS // 2)
        go(along(t, every, 0, 1))
        go(along(t, every, 1, -1))
        swap(fa.at[t], fa.at[t], 5)
        ga = Gather(
            ("x", "z"), lambda idx, rows: Wa.at[idx["z"], idx["x"], rows], (0, 192, 384),
            lambda ph, st, way: asend.at[ph, st, way], lambda ph, st, way: arecv.at[ph, st, way], pending,
        )
        go_ = Gather(
            ("y", "z", "x"), lambda idx, rows: Wo.at[idx["y"], idx["z"], idx["x"], rows], (0, 64, 128),
            lambda ph, st, way: osend.at[ph, st, way], lambda ph, st, way: orecv.at[ph, st, way], pending,
        )
        ga.begin(0)
        go_.begin(0)
        ga.pass_on(0)
        go_.pass_on(0)
        ga.finish(0)
        ga.begin(1)
        go_.finish(0)
        go_.begin(1)
        ga.pass_on(1)
        go_.pass_on(1)
        go_.finish(1)
        go_.begin(2)
        ga.finish(1)

        left, right, far = ((y + 3) % 4) * 2, ((y + 1) % 4) * 2, ((y + 2) % 4) * 2

        def widen(f, _):
            WaW[0:PROJ, pl.ds(pl.multiple_of(f * 128, 128), 128)] = Wa[f // 4, f % 4]
            return 0

        lax.fori_loop(0, 16, widen, 0)
        WaW[PROJ : PROJ + GR, :] = dd_ref[...]

        def project(pair):
            rows = fa[pl.ds(pair, 2)].reshape(2 * ROWS, D)
            proj[pl.ds(pl.multiple_of(pair * ROWS, 256), 256), 0 : PROJ + GR] = dot(rows, WaW[...], NT)

        across(fa.at[t], fa.at[t + 1 - 2 * c], 5).wait_recv()
        project(y * 2)
        along(left + c, every, 0, 1).wait_recv()
        go(along(left + c, low_half, 2, 1))
        swap(fa.at[left + c], fa.at[left + c], 6)
        along(right + c, every, 1, -1).wait_recv()
        go(along(right + c, high_half, 3, -1))
        swap(fa.at[right + c], fa.at[right + c], 7)
        go_.pass_on(2)
        across(fa.at[left + 1 - c], fa.at[left + 1 - c], 6).wait_recv()
        project(left)
        across(fa.at[right + 1 - c], fa.at[right + 1 - c], 7).wait_recv()
        project(right)
        along(far + c, low_half, 2, 1).wait_recv()
        along(far + c, high_half, 3, -1).wait_recv()
        swap(fa.at[far + c], fa.at[far + c], 8)
        across(fa.at[far + 1 - c], fa.at[far + 1 - c], 8).wait_recv()
        project(far)

        rowi = lax.broadcasted_iota(jnp.int32, (BLK, BLK), 0)
        coli = lax.broadcasted_iota(jnp.int32, (BLK, BLK), 1)
        tri = (rowi >= coli).astype(F32)

        def middle(b, size):
            if size >= 8:
                v = b.reshape(BLK // (2 * size), 2 * size, DK)[:, size - 1 : size, :]
                return jnp.broadcast_to(v, (BLK // (2 * size), 2 * size, DK)).reshape(BLK, DK)
            v = b.reshape(BLK // 8, 8, DK)
            sub = lax.broadcasted_iota(jnp.int32, (BLK // 8, 8, DK), 1)
            out = None
            for seg in range(8 // (2 * size)):
                at = seg * 2 * size + size - 1
                here = jnp.broadcast_to(v[:, at : at + 1, :], (BLK // 8, 8, DK))
                out = here if out is None else jnp.where(sub >= seg * 2 * size, here, out)
            return out.reshape(BLK, DK)

        def mix(i, state):
            rows = pl.ds(pl.multiple_of(i * BLK, BLK), BLK)
            p = proj[rows, :].astype(BF16)
            q = p[:, 0:64].astype(F32) * DK**-0.5
            k = p[:, 64:128].astype(F32)
            v = p[:, 128:256]
            pre = dot(p[:, PROJ : PROJ + GR], du_ref[...]) + bias_ref[...]
            lg = (jnp.minimum(pre, 0.0) - jnp.log1p(jnp.exp(-jnp.abs(pre)))) / GATE_DIVISOR
            b = dot(tri, lg, precision=lax.Precision.HIGHEST)
            scores = jnp.where(rowi == coli, jnp.sum(q * k, axis=1, keepdims=True), 0.0)
            size = 1
            while size < BLK:
                e = jnp.exp(-jnp.abs(b - middle(b, size)))
                s = dot((q * e).astype(BF16), (k * e).astype(BF16), NT)
                mask = (
                    (rowi // (2 * size) == coli // (2 * size))
                    & (rowi % (2 * size) >= size)
                    & (coli % (2 * size) < size)
                )
                scores = scores + jnp.where(mask, s, 0.0)
                size *= 2
            mixed = dot(scores.astype(BF16), v)
            mixed = mixed + dot((q * jnp.exp(b)).astype(BF16), state.astype(BF16), NT)
            last = b[BLK - 1 : BLK, :]
            state = state * jnp.exp(last) + dot(v, (k * jnp.exp(last - b)).astype(BF16), TN)
            normed = mixed * lax.rsqrt(jnp.mean(mixed * mixed, -1, keepdims=True) + HEAD_EPS) * gain_ref[...]
            gout[rows, :] = (normed * silu(p[:, 256:384].astype(F32))).astype(BF16)
            return state

        lax.fori_loop(0, 8, mix, jnp.zeros((DV, DK), F32))

        def home(step):
            to = (y + step) % 4
            return pltpu.make_async_remote_copy(
                src_ref=gout.at[pl.ds(pl.multiple_of(to * 256, 256), 256)], dst_ref=gin.at[y],
                send_sem=ysend.at[3 + step], recv_sem=yrecv.at[3 + step],
                device_id=neighbour("y", step), device_id_type=MESH,
            )

        for step in (2, 1, 3):
            go(home(step))
        gin[y] = gout[pl.ds(pl.multiple_of(y * 256, 256), 256), :]
        go_.finish(2)
        for step in (1, 3, 2):
            cp = pltpu.make_async_remote_copy(
                src_ref=gout.at[pl.ds(0, 256)], dst_ref=gin.at[(y + 4 - step) % 4],
                send_sem=ysend.at[3 + step], recv_sem=yrecv.at[3 + step],
                device_id=neighbour("y", step), device_id_type=MESH,
            )
            cp.wait_recv()

        def out_proj(j, _):
            weights = jnp.concatenate(
                [
                    jnp.concatenate([Wo[yy, j // 2, (j % 2) * 2 + i] for i in range(2)], axis=1)
                    for yy in range(4)
                ],
                axis=0,
            )
            cols = pl.ds(pl.multiple_of(j * 256, 256), 256)
            term = dot(jnp.concatenate([gin[yy] for yy in range(4)], axis=1), weights)
            acc[0, :, cols] = term[:ROWS]
            acc[1, :, cols] = term[ROWS:]
            return 0

        for cp in pending:
            cp.wait_send()
        pending.clear()
        lax.fori_loop(0, 8, out_proj, 0)
        swap(acc.at[1 - c], part.at[1], 3)
        xb[c] = joined(1, fa[t], RESIDUAL_SCALE, 1.0, 1)
        if stop == 2:
            out_ref[...] = xb[c]
        else:
            swap(xb.at[c], xb.at[c], 1)
            across(xb.at[1 - c], xb.at[1 - c], 1).wait_recv()
            for cp in pending:
                cp.wait_send()
            pending.clear()
            for ch in range(2):
                hidden(ch, xb)
                down(ch)
            swap(acc.at[1 - c], part.at[2], 4)
            out_ref[...] = joined(2, xb[c], RESIDUAL_SCALE, BRANCH_SCALE, 2)
    for cp in pending:
        cp.wait_send()


def on_device(
    stop, stream, gate_weight, up_weight, down_weight, query_weight, key_weight, value_weight, outgate_weight,
    decay_down, decay_up, decay_bias, head_gain, out_weight, norm_gain,
):
    vmem = pl.BlockSpec(memory_space=pltpu.VMEM)
    dma = pltpu.SemaphoreType.DMA
    return pl.pallas_call(
        functools.partial(kernel, stop),
        out_shape=jax.ShapeDtypeStruct((ROWS, D), BF16),
        in_specs=[vmem] * 14,
        out_specs=vmem,
        scratch_shapes=[
            pltpu.VMEM((3, 4, 4, 4, HID, 128), BF16),
            pltpu.VMEM((4, 4, PROJ, 128), BF16),
            pltpu.VMEM((4, 4, 4, 128, 128), BF16),
            pltpu.VMEM((PROJ + GR, D), BF16),
            pltpu.VMEM((2, ROWS, D), BF16),
            pltpu.VMEM((2, ROWS, D), BF16),
            pltpu.VMEM((768, 256), F32),
            pltpu.VMEM((256, 768), BF16),
            pltpu.VMEM((2, ROWS, D), F32),
            pltpu.VMEM((3, ROWS, D), F32),
            pltpu.VMEM((8, ROWS, D), BF16),
            pltpu.VMEM((1024, 512), F32),
            pltpu.VMEM((1024, DV), BF16),
            pltpu.VMEM((4, 256, DV), BF16),
            dma((5,)),
            dma((2, 3, 3, 2, 2)),
            dma((2, 3, 3, 2, 2)),
            dma((2, 2, 2)),
            dma((2, 2, 2)),
            dma((3, 2, 2)),
            dma((3, 2, 2)),
            dma((9,)),
            dma((9,)),
            dma((7,)),
            dma((7,)),
        ],
        compiler_params=pltpu.CompilerParams(
            collective_id=0, has_side_effects=True, vmem_limit_bytes=60 * 1024 * 1024
        ),
    )(
        stream, gate_weight.T, up_weight.T, down_weight, query_weight.T, key_weight.T, value_weight, outgate_weight,
        decay_down.T, decay_up, decay_bias[None], head_gain[None], out_weight, norm_gain,
    )


def solution(mesh, stop=0):
    in_specs = (
        P(("rep", "fs", "tp"), None),
        P("fs", "tp"),
        P("fs", "tp"),
        P("tp", "fs"),
        P("fs", "tp"),
        P("fs", "tp"),
        P("fs", "tp"),
        P("fs", "tp"),
        P(),
        P(None, "tp"),
        P("tp"),
        P(),
        P("tp", "fs"),
        P(),
    )
    return jax.shard_map(
        functools.partial(on_device, stop),
        mesh=mesh,
        in_specs=in_specs,
        out_specs=P(("rep", "fs", "tp"), None),
        check_vma=False,
    )
```

time: 474 us -> 176 us (0.37)
  waiting for transfers between devices: 277 us -> 0 us
  Pallas kernels: 0 us -> 174 us
  blocking collectives: 71.8 us -> 0 us
  matrix products: 52.6 us -> 0 us
  other arithmetic: 34.7 us -> 0 us
  starting transfers between devices: 14.7 us -> 0 us
  between operations: 13.8 us -> 0.01 us
  local copies, waits for them, and re-layouts: 8.37 us -> 1.88 us
    all_gather x7 -> x0, waiting for transfers between devices: 237 us -> none  [the longest x2 79.9 us: ffn_half(): gathered = lax.all_gather(current, 'tp', axis=0, tiled=True)]
    pallas_call x0 -> x1, Pallas kernels: none -> 174 us  [on_device(): pl.pallas_call(functools.partial(kernel, stop), out_shape=jax.ShapeDtypeS...]
    all_to_all x2 -> x0, blocking collectives: 71.8 us -> none  [the longest x1 57.1 us: from_everyone(): return lax.all_to_all(copies, axis, split_axis=0, concat_axis=0, tiled=True)]
    dot_general x60 -> x0, matrix products: 52.6 us -> none  [the longest x4 14.7 us: on_device(): jnp.dot(gathered, piece, preferred_element_type=jnp.float32)]
    all_to_all x3 -> x0, waiting for transfers between devices: 38.7 us -> none  [the longest x1 17.3 us: from_everyone(): return lax.all_to_all(copies, axis, split_axis=0, concat_axis=0, tiled=True)]
    reduce_sum x20 -> x0, other arithmetic: 22.7 us -> none  [the longest x16 21.7 us: advance(): jnp.sum(query_blk[:, :, None, :] * key_blk[:, None, :, :] * jnp.exp(log_g...]
    all_to_all x3 -> x0, starting transfers between devices: 14.3 us -> none  [the longest x1 7.04 us: from_everyone(): return lax.all_to_all(copies, axis, split_axis=0, concat_axis=0, tiled=True)]
    another operation x1 -> x0, other arithmetic: 6.33 us -> none  [blocked_mixer(): cumulative = jnp.cumsum(split_blocks(log_gate), axis=2)]
  transfers between devices with their start and end apart: 10 -> 0, of which waited for: 9 -> 0; matrix products, arithmetic and copies ran while one was open for 16% -> 0% of each run, Pallas kernels for 0% -> 0%
where the time goes in v1:
time: 176 us
  Pallas kernels  174 us (99%)
  local copies, waits for them, and re-layouts  1.88 us (1%)
    pallas_call x1, Pallas kernels, on_device(): pl.pallas_call(functools.partial(kernel, stop), out_shape=jax.ShapeDtypeS...  174 us

profile of v1, /device:TPU:1, one launch (start us, length us, event | category | flops | bytes accessed | tf_op | source)
XLA Modules:
  0.0 175.7 jit_solution(9267981089412315030)
XLA Ops:
  0.0 173.8 %shard_map.136 = bf16[128,2048]{1,0:T(8,128)(2,1)} custom-call(bf16[128,2048]{1,0:T(8,128)(2,1)} %x_ref.1, bf16[352,128]{1,0:T(8,128)(2,1)} %bitcast.8, bf16[352,128]{1,0:T(8,128)(2,1)} %bitcast.9, bf16[352,128]{1,0:T(8,128)(2,1)} %d_ref.1, bf16[64,128]{1,0:T(8,128)(2,1)} %bitcast.10, bf16[64,128]{1,0:T(8,128)(2,1)} %bitcast.11, bf16[128,128]{1,0:T(8,128)(2,1)} %v_ref.1, ...), custom_call_target="tpu_custom_call" | custom-call | tf_op jit(solution)/shard_map/pallas_call | solution.py:429
  173.8 1.9 %copy.16 = bf16[128,2048]{1,0:T(8,128)(2,1)} copy(bf16[128,2048]{1,0:T(8,128)(2,1)} %shard_map.136) | data formatting | bytes 1048576

commit v2 on v1

v2 whole, which is shorter than its diff:
```python
import functools

import jax
import jax.numpy as jnp
from jax import lax
from jax.experimental import pallas as pl
from jax.experimental.pallas import tpu as pltpu
from jax.sharding import PartitionSpec as P

MESH = pl.DeviceIdType.MESH
F32, BF16 = jnp.float32, jnp.bfloat16
D, DK, DV, GR = 2048, 64, 128, 32
ROWS = 128
HID = 352
CHUNKS = ((0, 32, 64), (64, 160, 256), (256, 304, 352))
SECOND = ((0, HID),)
PROJ = 384
BLK = 128
RESIDUAL_SCALE = 2.0**0.5
BRANCH_SCALE = 0.5
NORM_EPS = 1e-05
HEAD_EPS = 0.01
GATE_DIVISOR = 16.0

NT = (((1,), (1,)), ((), ()))
NN = (((1,), (0,)), ((), ()))
TN = (((0,), (0,)), ((), ()))


def dot(a, b, dims=NN, **kw):
    return lax.dot_general(a, b, dims, preferred_element_type=F32, **kw)


def place():
    r, f, t = lax.axis_index("rep"), lax.axis_index("fs"), lax.axis_index("tp")
    return r, f // 4, f % 4, t // 2, t % 2


def neighbour(dim, step):
    r, zl, x, y, c = place()
    if dim == "x":
        return (r, zl * 4 + (x + step + 4) % 4, y * 2 + c)
    if dim == "y":
        return (r, zl * 4 + x, ((y + step + 4) % 4) * 2 + c)
    if dim == "c":
        return (r, zl * 4 + x, y * 2 + 1 - c)
    z = (r * 4 + zl + step + 8) % 8
    return (z // 4, (z % 4) * 4 + x, y * 2 + c)


class Gather:
    def __init__(self, order, at, rows, send, recv, pending):
        self.order, self.at, self.rows = order, at, rows
        self.send, self.recv, self.pending = send, recv, pending
        r, zl, x, y, c = place()
        self.pos = {"x": x, "y": y, "z": zl}

    def region(self, phase, shift, half):
        lo, mid, hi = self.rows
        lo, hi = ((lo, mid), (mid, hi))[half]
        idx = {}
        for k, dim in enumerate(self.order):
            if k < phase:
                idx[dim] = slice(None)
            elif k == phase:
                idx[dim] = (self.pos[dim] + shift) % 4
            else:
                idx[dim] = self.pos[dim]
        return self.at(idx, pl.ds(lo, hi - lo))

    def copy(self, phase, shift, half, stage, way):
        region = self.region(phase, shift, half)
        return pltpu.make_async_remote_copy(
            src_ref=region,
            dst_ref=region,
            send_sem=self.send(phase, stage, way),
            recv_sem=self.recv(phase, stage, way),
            device_id=neighbour(self.order[phase], 1 if way == 0 else -1),
            device_id_type=MESH,
        )

    def go(self, *args):
        cp = self.copy(*args)
        cp.start()
        self.pending.append(cp)

    def begin(self, phase):
        for stage in (0, 1):
            for way in (0, 1):
                self.go(phase, 0, way ^ stage, stage, way)

    def pass_on(self, phase):
        for way in (0, 1):
            self.copy(phase, 3 - 2 * way, way, 0, way).wait_recv()
        for way in (0, 1):
            self.go(phase, 3 - 2 * way, way, 2, way)

    def finish(self, phase):
        for way in (0, 1):
            self.copy(phase, 3 - 2 * way, 1 - way, 1, way).wait_recv()
        for way in (0, 1):
            self.copy(phase, 2, way, 2, way).wait_recv()


def layer_norm(values, norm_scale):
    average = jnp.mean(values, -1, keepdims=True)
    centred = values - average
    spread = jnp.mean(centred * centred, -1, keepdims=True)
    return (centred * lax.rsqrt(spread + NORM_EPS) * norm_scale).astype(BF16)


scope = jax.named_scope


def silu(v):
    return v / (1.0 + jnp.exp(-v))


def kernel(
    stop,
    x_ref, g_ref, u_ref, d_ref, q_ref, k_ref, v_ref, og_ref, dd_ref, du_ref, bias_ref, gain_ref, wo_ref, norm_ref,
    out_ref,
    W, Wa, Wo, WaW, xa, xb, xs, hidT, hid, acc, part, fa, proj, inner, qe, upd, shrink, level, gout, gin,
    lsem, fsend, frecv, asend, arecv, osend, orecv, csend, crecv, ysend, yrecv, hsend, hrecv,
):
    r, zl, x, y, c = place()
    t = y * 2 + c
    barrier = pltpu.get_barrier_semaphore()
    for dim in "xyz":
        for step in (1, -1):
            pl.semaphore_signal(barrier, 1, device_id=neighbour(dim, step), device_id_type=MESH)
    pl.semaphore_signal(barrier, 1, device_id=neighbour("c", 1), device_id_type=MESH)
    pl.semaphore_signal(barrier, 1, device_id=neighbour("y", 2), device_id_type=MESH)
    own = []
    for w, ref in enumerate((g_ref, u_ref, d_ref)):
        own.append(pltpu.make_async_copy(ref, W.at[w, y, zl, x], lsem.at[w]))
    own.append(pltpu.make_async_copy(wo_ref, Wo.at[y, zl, x], lsem.at[3]))
    for cp in own:
        cp.start()
    with scope("barrier"):
        pl.semaphore_wait(barrier, 8)
        for cp in own:
            cp.wait()

    pending = []

    def go(cp):
        cp.start()
        pending.append(cp)

    def settle():
        for cp in pending:
            cp.wait_send()
        pending.clear()

    def across(src, dst, slot):
        return pltpu.make_async_remote_copy(
            src_ref=src, dst_ref=dst, send_sem=csend.at[slot], recv_sem=crecv.at[slot],
            device_id=neighbour("c", 1), device_id_type=MESH,
        )

    orders = (("x", "z", "y"), ("z", "y", "x"), ("y", "x", "z"))

    def ffn_gather(ch, w):
        return Gather(
            orders[w],
            lambda idx, rows: W.at[w, idx["y"], idx["z"], idx["x"], rows],
            CHUNKS[ch],
            lambda ph, st, way: fsend.at[ch, w, ph, st, way],
            lambda ph, st, way: frecv.at[ch, w, ph, st, way],
            pending,
        )

    ffn = [[ffn_gather(ch, w) for w in range(3)] for ch in range(3)]
    ga = Gather(
        ("x", "z"), lambda idx, rows: Wa.at[idx["z"], idx["x"], rows], (0, 192, 384),
        lambda ph, st, way: asend.at[ph, st, way], lambda ph, st, way: arecv.at[ph, st, way], pending,
    )
    gw = Gather(
        ("y", "x", "z"), lambda idx, rows: Wo.at[idx["y"], idx["z"], idx["x"], rows], (0, 64, 128),
        lambda ph, st, way: osend.at[ph, st, way], lambda ph, st, way: orecv.at[ph, st, way], pending,
    )

    def begin(ch, ph):
        with scope(f"begin{ch}_{ph}"):
            for w in range(3):
                if ph:
                    ffn[ch][w].finish(ph - 1)
                ffn[ch][w].begin(ph)

    def pass_on(ch, ph):
        with scope(f"pass{ch}_{ph}"):
            for w in range(3):
                ffn[ch][w].pass_on(ph)

    def hidden(lo, hi, rows):
        size = hi - lo

        def body(yy, _):
            gate, up = (
                dot(
                    jnp.concatenate([W[w, yy, f // 4, f % 4, lo:hi, :] for f in range(16)], axis=1),
                    jnp.concatenate([rows[0], rows[1]], axis=1),
                )
                for w in (0, 1)
            )
            hidT[pl.ds(pl.multiple_of(yy * size, 16), size), :] = silu(gate) * up
            return 0

        lax.fori_loop(0, 4, body, 0, unroll=2)
        hid[:, : 4 * size] = hidT[: 4 * size, :].T.astype(BF16)

    def down(lo, hi, slot):
        size = hi - lo

        def body(j, _):
            weights = jnp.concatenate(
                [
                    jnp.concatenate([W[2, yy, j // 2, (j % 2) * 2 + i, lo:hi, :] for i in range(2)], axis=1)
                    for yy in range(4)
                ],
                axis=0,
            )
            cols = pl.ds(pl.multiple_of(j * 256, 256), 256)
            term = dot(hid[:, : 4 * size], weights)
            for half in range(2):
                piece = term[half * ROWS : (half + 1) * ROWS]
                if lo:
                    acc[half, :, cols] += piece
                else:
                    acc[half, :, cols] = piece
            return 0

        if hi == HID:
            halves(body, slot)
        else:
            lax.fori_loop(0, 8, body, 0, unroll=2)

    def give(slot, half):
        cols = pl.ds(half * 1024, 1024)
        return across(acc.at[1 - c, :, cols], part.at[slot, :, cols], 2 + 2 * slot + half)

    def halves(body, slot):
        for half in range(2):
            lax.fori_loop(half * 4, half * 4 + 4, body, 0, unroll=2)
            go(give(slot, half))

    def joined(slot, residual, scale, branch, norm):
        with scope(f"swap_{slot}"):
            for half in range(2):
                give(slot, half).wait_recv()
        with scope(f"norm_{slot}"):
            total = acc[c] + part[slot]
            return layer_norm(scale * residual.astype(F32) + branch * total, norm_ref[norm : norm + 1, :])

    for ch in range(3):
        begin(ch, 0)
    Wa[zl, x, 0:64, :] = q_ref[...]
    Wa[zl, x, 64:128, :] = k_ref[...]
    Wa[zl, x, 128:256, :] = v_ref[...].astype(F32).T.astype(BF16)
    Wa[zl, x, 256:384, :] = og_ref[...].astype(F32).T.astype(BF16)
    pass_on(0, 0)
    pass_on(1, 0)
    begin(0, 1)
    pass_on(2, 0)
    begin(1, 1)
    ga.begin(0)
    gw.begin(0)
    pass_on(0, 1)
    begin(2, 1)
    begin(0, 2)
    pass_on(1, 1)
    ga.pass_on(0)
    gw.pass_on(0)
    pass_on(2, 1)
    xa[c] = x_ref[...].astype(F32).T.astype(BF16)
    go(across(xa.at[c], xa.at[c], 0))
    pass_on(0, 2)
    begin(1, 2)
    rowi = lax.broadcasted_iota(jnp.int32, (BLK, BLK), 0)
    coli = lax.broadcasted_iota(jnp.int32, (BLK, BLK), 1)
    differ = jnp.bitwise_xor(rowi, coli)
    bits = jnp.zeros((BLK, BLK), jnp.int32)
    for k in range(7):
        bits = bits + (differ >= 2**k).astype(jnp.int32)
    level[...] = jnp.where(rowi >= coli, bits, -1)
    WaW[PROJ : PROJ + GR, :] = dd_ref[...]

    def ffn_compute(span, rows, slot):
        with scope(f"hidden{span[0]}"):
            hidden(*span, rows)
        with scope(f"down{span[0]}"):
            down(*span, slot)

    def finish(ch):
        with scope(f"finish{ch}"):
            for w in range(3):
                ffn[ch][w].finish(2)

    across(xa.at[c], xa.at[c], 0).wait_recv()
    finish(0)
    ffn_compute((0, 64), xa, 0)
    pass_on(1, 2)
    begin(2, 2)
    finish(1)
    ffn_compute((64, 256), xa, 0)
    pass_on(2, 2)
    ga.finish(0)
    ga.begin(1)
    gw.finish(0)
    gw.begin(1)
    finish(2)
    ffn_compute((256, HID), xa, 0)
    fa[t] = joined(0, x_ref[...], RESIDUAL_SCALE, BRANCH_SCALE, 0)

    half_rows = (pl.ds(0, ROWS // 2), pl.ds(ROWS // 2, ROWS // 2))

    def along(block, half, stage, way):
        ref = fa.at[block, half_rows[half]]
        return pltpu.make_async_remote_copy(
            src_ref=ref, dst_ref=ref, send_sem=ysend.at[stage, way], recv_sem=yrecv.at[stage, way],
            device_id=neighbour("y", 1 - 2 * way), device_id_type=MESH,
        )

    for stage in (0, 1):
        for way in (0, 1):
            go(along(t, way ^ stage, stage, way))

    def share(block, slot):
        return across(fa.at[block], fa.at[block], 8 + slot)

    go(share(t, 0))
    side = [((y + 3) % 4) * 2, ((y + 1) % 4) * 2]
    far = ((y + 2) % 4) * 2

    with scope("attention2"):
        ga.pass_on(1)
    with scope("attention2b"):
        gw.pass_on(1)
    with scope("rows0"):
        for way in (0, 1):
            along(side[way] + c, way, 0, way).wait_recv()
            go(along(side[way] + c, way, 2, way))
    with scope("attention3"):
        ga.finish(1)

    def widen(f, _):
        WaW[0:PROJ, pl.ds(pl.multiple_of(f * 128, 128), 128)] = Wa[f // 4, f % 4]
        return 0

    with scope("widen"):
        lax.fori_loop(0, 16, widen, 0)
    with scope("attention4"):
        gw.finish(1)
        gw.begin(2)

    def middle(b, size):
        if size >= 8:
            v = b.reshape(BLK // (2 * size), 2 * size, DK)[:, size - 1 : size, :]
            return jnp.broadcast_to(v, (BLK // (2 * size), 2 * size, DK)).reshape(BLK, DK)
        v = b.reshape(BLK // 8, 8, DK)
        sub = lax.broadcasted_iota(jnp.int32, (BLK // 8, 8, DK), 1)
        out = None
        for seg in range(8 // (2 * size)):
            at = seg * 2 * size + size - 1
            here = jnp.broadcast_to(v[:, at : at + 1, :], (BLK // 8, 8, DK))
            out = here if out is None else jnp.where(sub >= seg * 2 * size, here, out)
        return out.reshape(BLK, DK)

    def within(i):
        rows = pl.ds(pl.multiple_of(i * BLK, BLK), BLK)
        p = proj[rows, :].astype(BF16)
        q = p[:, 0:64].astype(F32) * DK**-0.5
        k = p[:, 64:128].astype(F32)
        v = p[:, 128:256]
        pre = dot(p[:, PROJ : PROJ + GR], du_ref[...]) + bias_ref[...]
        lg = (jnp.minimum(pre, 0.0) - jnp.log1p(jnp.exp(-jnp.abs(pre)))) / GATE_DIVISOR
        tri = (level[...] >= 0).astype(F32)
        b = dot(tri, lg, precision=lax.Precision.HIGHEST)
        lev = level[...]
        scores = jnp.where(lev == 0, jnp.sum(q * k, axis=1, keepdims=True), 0.0)
        for n in range(7):
            e = jnp.exp(-jnp.abs(b - middle(b, 2**n)))
            s = dot((q * e).astype(BF16), (k * e).astype(BF16), NT)
            scores = jnp.where(lev == n + 1, s, scores)
        inner[rows, :] = dot(scores.astype(BF16), v)
        qe[rows, :] = (q * jnp.exp(b)).astype(BF16)
        last = b[BLK - 1 : BLK, :]
        shrink[i] = jnp.exp(last)
        upd[i] = dot(v, (k * jnp.exp(last - b)).astype(BF16), TN)

    def project(pair):
        with scope("project"):
            rows = fa[pl.ds(pair, 2)].reshape(2 * ROWS, D)
            proj[pl.ds(pl.multiple_of(pair * ROWS, 256), 256), 0 : PROJ + GR] = dot(rows, WaW[...], NT)
        with scope("within"):
            within(pair)
            within(pair + 1)

    share(t + 1 - 2 * c, 0).wait_recv()
    project(y * 2)
    with scope("rows1"):
        for way in (0, 1):
            along(side[way] + c, 1 - way, 1, way).wait_recv()
            go(share(side[way] + c, 1 + way))
    share(side[0] + 1 - c, 1).wait_recv()
    project(side[0])
    with scope("rows2"):
        share(side[1] + 1 - c, 2).wait_recv()
    project(side[1])
    with scope("attention5"):
        gw.pass_on(2)
    with scope("rows2b"):
        for way in (0, 1):
            along(far + c, way, 2, way).wait_recv()
        go(share(far + c, 3))
    with scope("rows3"):
        share(far + 1 - c, 3).wait_recv()
    project(far)

    def home(to):
        return pltpu.make_async_remote_copy(
            src_ref=gout.at[pl.ds(to * 256, 256)], dst_ref=gin.at[y],
            send_sem=hsend.at[to], recv_sem=hrecv.at[y],
            device_id=(r, zl * 4 + x, to * 2 + c), device_id_type=MESH,
        )

    state = jnp.zeros((DV, DK), F32)
    with scope("scan"):
        for i in range(8):
            rows = pl.ds(i * BLK, BLK)
            mixed = inner[rows, :] + dot(qe[rows, :], state.astype(BF16), NT)
            state = state * shrink[i] + upd[i]
            normed = mixed * lax.rsqrt(jnp.mean(mixed * mixed, -1, keepdims=True) + HEAD_EPS) * gain_ref[...]
            gate = proj[rows, 256:384].astype(BF16).astype(F32)
            gout[rows, :] = (normed * silu(gate)).astype(BF16)
            if i % 2:

                @pl.when(y != i // 2)
                def _():
                    home(i // 2).start()

                @pl.when(y == i // 2)
                def _():
                    gin[i // 2] = gout[(i - 1) * BLK : (i + 1) * BLK, :]

    with scope("wo"):
        gw.finish(2)
    settle()
    with scope("home"):
        for step in range(1, 4):
            source = (y + step) % 4
            pltpu.make_async_remote_copy(
                src_ref=gout.at[pl.ds(0, 256)], dst_ref=gin.at[source],
                send_sem=hsend.at[source], recv_sem=hrecv.at[source],
                device_id=(r, zl * 4 + x, source * 2 + c), device_id_type=MESH,
            ).wait()

    def out_proj(j, _):
        weights = jnp.concatenate(
            [jnp.concatenate([Wo[yy, j // 2, (j % 2) * 2 + i] for i in range(2)], axis=1) for yy in range(4)],
            axis=0,
        )
        cols = pl.ds(pl.multiple_of(j * 256, 256), 256)
        term = dot(jnp.concatenate([gin[yy] for yy in range(4)], axis=1), weights)
        acc[0, :, cols] = term[:ROWS]
        acc[1, :, cols] = term[ROWS:]
        return 0

    with scope("outp"):
        halves(out_proj, 1)
    second = joined(1, fa[t], RESIDUAL_SCALE, 1.0, 1)
    xs[...] = second
    xb[c] = second.astype(F32).T.astype(BF16)
    go(across(xb.at[c], xb.at[c], 1))
    with scope("swapx"):
        across(xb.at[1 - c], xb.at[1 - c], 1).wait_recv()
    settle()
    for span in SECOND:
        ffn_compute(span, xb, 2)
    out_ref[...] = joined(2, xs[...], RESIDUAL_SCALE, BRANCH_SCALE, 2)
    if stop == 1:
        out_ref[...] = fa[t]
    if stop == 2:
        out_ref[...] = xs[...]
    settle()


def on_device(
    stop, stream, gate_weight, up_weight, down_weight, query_weight, key_weight, value_weight, outgate_weight,
    decay_down, decay_up, decay_bias, head_gain, out_weight, norm_gain,
):
    vmem = pl.BlockSpec(memory_space=pltpu.VMEM)
    dma = pltpu.SemaphoreType.DMA
    return pl.pallas_call(
        functools.partial(kernel, stop),
        out_shape=jax.ShapeDtypeStruct((ROWS, D), BF16),
        in_specs=[vmem] * 14,
        out_specs=vmem,
        scratch_shapes=[
            pltpu.VMEM((3, 4, 4, 4, HID, 128), BF16),
            pltpu.VMEM((4, 4, PROJ, 128), BF16),
            pltpu.VMEM((4, 4, 4, 128, 128), BF16),
            pltpu.VMEM((PROJ + GR, D), BF16),
            pltpu.VMEM((2, D, ROWS), BF16),
            pltpu.VMEM((2, D, ROWS), BF16),
            pltpu.VMEM((ROWS, D), BF16),
            pltpu.VMEM((4 * HID, 256), F32),
            pltpu.VMEM((256, 4 * HID), BF16),
            pltpu.VMEM((2, ROWS, D), F32),
            pltpu.VMEM((3, ROWS, D), F32),
            pltpu.VMEM((8, ROWS, D), BF16),
            pltpu.VMEM((1024, 512), F32),
            pltpu.VMEM((1024, DV), F32),
            pltpu.VMEM((1024, DK), BF16),
            pltpu.VMEM((8, DV, DK), F32),
            pltpu.VMEM((8, 1, DK), F32),
            pltpu.VMEM((BLK, BLK), jnp.int32),
            pltpu.VMEM((1024, DV), BF16),
            pltpu.VMEM((4, 256, DV), BF16),
            dma((4,)),
            dma((3, 3, 3, 3, 2)),
            dma((3, 3, 3, 3, 2)),
            dma((2, 3, 2)),
            dma((2, 3, 2)),
            dma((3, 3, 2)),
            dma((3, 3, 2)),
            dma((12,)),
            dma((12,)),
            dma((3, 2)),
            dma((3, 2)),
            dma((4,)),
            dma((4,)),
        ],
        compiler_params=pltpu.CompilerParams(
            collective_id=0, has_side_effects=True, vmem_limit_bytes=60 * 1024 * 1024
        ),
    )(
        stream, gate_weight.T, up_weight.T, down_weight, query_weight.T, key_weight.T, value_weight, outgate_weight,
        decay_down.T, decay_up, decay_bias[None], head_gain[None], out_weight, norm_gain,
    )


def solution(mesh, stop=0):
    in_specs = (
        P(("rep", "fs", "tp"), None),
        P("fs", "tp"),
        P("fs", "tp"),
        P("tp", "fs"),
        P("fs", "tp"),
        P("fs", "tp"),
        P("fs", "tp"),
        P("fs", "tp"),
        P(),
        P(None, "tp"),
        P("tp"),
        P(),
        P("tp", "fs"),
        P(),
    )
    return jax.shard_map(
        functools.partial(on_device, stop),
        mesh=mesh,
        in_specs=in_specs,
        out_specs=P(("rep", "fs", "tp"), None),
        check_vma=False,
    )
```

time: 176 us -> 136 us (0.77)
  Pallas kernels: 174 us -> 134 us
    pallas_call x1, Pallas kernels: 174 us -> 134 us  [on_device(): pl.pallas_call(functools.partial(kernel, stop), out_shape=jax.ShapeDtypeS...]
where the time goes in v2:
time: 136 us
  Pallas kernels  134 us (99%)
  local copies, waits for them, and re-layouts  1.88 us (1%)
    pallas_call x1, Pallas kernels, on_device(): pl.pallas_call(functools.partial(kernel, stop), out_shape=jax.ShapeDtypeS...  134 us

profile of v2, /device:TPU:1, one launch (start us, length us, event | category | flops | bytes accessed | tf_op | source)
XLA Modules:
  0.0 135.6 jit_solution(8266733285161341659)
XLA Ops:
  0.0 133.7 %shard_map.136 = bf16[128,2048]{1,0:T(8,128)(2,1)} custom-call(bf16[128,2048]{1,0:T(8,128)(2,1)} %x_ref.1, bf16[352,128]{1,0:T(8,128)(2,1)} %bitcast.8, bf16[352,128]{1,0:T(8,128)(2,1)} %bitcast.9, bf16[352,128]{1,0:T(8,128)(2,1)} %d_ref.1, bf16[64,128]{1,0:T(8,128)(2,1)} %bitcast.10, bf16[64,128]{1,0:T(8,128)(2,1)} %bitcast.11, bf16[128,128]{1,0:T(8,128)(2,1)} %v_ref.1, ...), custom_call_target="tpu_custom_call" | custom-call | tf_op jit(solution)/shard_map/pallas_call | solution.py:495
  133.7 1.9 %copy.16 = bf16[128,2048]{1,0:T(8,128)(2,1)} copy(bf16[128,2048]{1,0:T(8,128)(2,1)} %shard_map.136) | data formatting | bytes 1048576

commit v3 on v2

--- a/solution.py
+++ b/solution.py
@@ -15,6 +15,7 @@
 CHUNKS = ((0, 32, 64), (64, 160, 256), (256, 304, 352))
 SECOND = ((0, HID),)
 PROJ = 384
+VMEM_LIMIT = 60 * 1024 * 1024
 BLK = 128
 RESIDUAL_SCALE = 2.0**0.5
 BRANCH_SCALE = 0.5
@@ -120,7 +121,8 @@
     stop,
     x_ref, g_ref, u_ref, d_ref, q_ref, k_ref, v_ref, og_ref, dd_ref, du_ref, bias_ref, gain_ref, wo_ref, norm_ref,
     out_ref,
-    W, Wa, Wo, WaW, xa, xb, xs, hidT, hid, acc, part, fa, proj, inner, qe, upd, shrink, level, gout, gin,
+    W, Wa, Wo, WaW, xa, xb, xs, hidT, hid, acc, part, fa, proj, inner, qe, upd, shrink, gate, du2, bias2, level,
+    gout, gin,
     lsem, fsend, frecv, asend, arecv, osend, orecv, csend, crecv, ysend, yrecv, hsend, hrecv,
 ):
     r, zl, x, y, c = place()
@@ -172,14 +174,26 @@
         )
 
     ffn = [[ffn_gather(ch, w) for w in range(3)] for ch in range(3)]
-    ga = Gather(
-        ("x", "z"), lambda idx, rows: Wa.at[idx["z"], idx["x"], rows], (0, 192, 384),
-        lambda ph, st, way: asend.at[ph, st, way], lambda ph, st, way: arecv.at[ph, st, way], pending,
-    )
-    gw = Gather(
-        ("y", "x", "z"), lambda idx, rows: Wo.at[idx["y"], idx["z"], idx["x"], rows], (0, 64, 128),
-        lambda ph, st, way: osend.at[ph, st, way], lambda ph, st, way: orecv.at[ph, st, way], pending,
-    )
+    ga = [
+        Gather(
+            order, lambda idx, rows: Wa.at[idx["z"], idx["x"], rows], span,
+            lambda ph, st, way, n=n: asend.at[n, ph, st, way], lambda ph, st, way, n=n: arecv.at[n, ph, st, way],
+            pending,
+        )
+        for n, (order, span) in enumerate(((("x", "z"), (0, 96, 192)), (("z", "x"), (192, 288, 384))))
+    ]
+    gw = [
+        Gather(
+            order, lambda idx, rows: Wo.at[idx["y"], idx["z"], idx["x"], rows], span,
+            lambda ph, st, way, n=n: osend.at[n, ph, st, way], lambda ph, st, way, n=n: orecv.at[n, ph, st, way],
+            pending,
+        )
+        for n, (order, span) in enumerate(((("y", "x", "z"), (0, 32, 64)), (("y", "z", "x"), (64, 96, 128))))
+    ]
+
+    def each(gathers, op, phase):
+        for g in gathers:
+            getattr(g, op)(phase)
 
     def begin(ch, ph):
         with scope(f"begin{ch}_{ph}"):
@@ -207,7 +221,7 @@
             hidT[pl.ds(pl.multiple_of(yy * size, 16), size), :] = silu(gate) * up
             return 0
 
-        lax.fori_loop(0, 4, body, 0, unroll=2)
+        lax.fori_loop(0, 4, body, 0, unroll=True)
         hid[:, : 4 * size] = hidT[: 4 * size, :].T.astype(BF16)
 
     def down(lo, hi, slot):
@@ -232,23 +246,23 @@
             return 0
 
         if hi == HID:
-            halves(body, slot)
+            pieces(body, slot)
         else:
             lax.fori_loop(0, 8, body, 0, unroll=2)
 
-    def give(slot, half):
-        cols = pl.ds(half * 1024, 1024)
-        return across(acc.at[1 - c, :, cols], part.at[slot, :, cols], 2 + 2 * slot + half)
-
-    def halves(body, slot):
-        for half in range(2):
-            lax.fori_loop(half * 4, half * 4 + 4, body, 0, unroll=2)
-            go(give(slot, half))
+    def give(slot, piece):
+        cols = pl.ds(piece * 512, 512)
+        return across(acc.at[1 - c, :, cols], part.at[slot, :, cols], 2 + 4 * slot + piece)
+
+    def pieces(body, slot):
+        for piece in range(4):
+            lax.fori_loop(piece * 2, piece * 2 + 2, body, 0, unroll=True)
+            go(give(slot, piece))
 
     def joined(slot, residual, scale, branch, norm):
         with scope(f"swap_{slot}"):
-            for half in range(2):
-                give(slot, half).wait_recv()
+            for piece in range(4):
+                give(slot, piece).wait_recv()
         with scope(f"norm_{slot}"):
             total = acc[c] + part[slot]
             return layer_norm(scale * residual.astype(F32) + branch * total, norm_ref[norm : norm + 1, :])
@@ -264,19 +278,22 @@
     begin(0, 1)
     pass_on(2, 0)
     begin(1, 1)
-    ga.begin(0)
-    gw.begin(0)
+    each(ga, "begin", 0)
+    each(gw, "begin", 0)
     pass_on(0, 1)
     begin(2, 1)
     begin(0, 2)
     pass_on(1, 1)
-    ga.pass_on(0)
-    gw.pass_on(0)
+    each(ga, "pass_on", 0)
+    each(gw, "pass_on", 0)
     pass_on(2, 1)
     xa[c] = x_ref[...].astype(F32).T.astype(BF16)
     go(across(xa.at[c], xa.at[c], 0))
     pass_on(0, 2)
     begin(1, 2)
+    for half in range(2):
+        du2[:, half * DK : (half + 1) * DK] = du_ref[...]
+        bias2[:, half * DK : (half + 1) * DK] = bias_ref[...]
     rowi = lax.broadcasted_iota(jnp.int32, (BLK, BLK), 0)
     coli = lax.broadcasted_iota(jnp.int32, (BLK, BLK), 1)
     differ = jnp.bitwise_xor(rowi, coli)
@@ -305,10 +322,10 @@
     finish(1)
     ffn_compute((64, 256), xa, 0)
     pass_on(2, 2)
-    ga.finish(0)
-    ga.begin(1)
-    gw.finish(0)
-    gw.begin(1)
+    each(ga, "finish", 0)
+    each(ga, "begin", 1)
+    each(gw, "finish", 0)
+    each(gw, "begin", 1)
     finish(2)
     ffn_compute((256, HID), xa, 0)
     fa[t] = joined(0, x_ref[...], RESIDUAL_SCALE, BRANCH_SCALE, 0)
@@ -326,23 +343,29 @@
         for way in (0, 1):
             go(along(t, way ^ stage, stage, way))
 
-    def share(block, slot):
-        return across(fa.at[block], fa.at[block], 8 + slot)
-
-    go(share(t, 0))
+    def share(block, half, slot):
+        ref = fa.at[block, half_rows[half]]
+        return across(ref, ref, 14 + 2 * slot + half)
+
+    go(share(t, 0, 0))
+    go(share(t, 1, 0))
     side = [((y + 3) % 4) * 2, ((y + 1) % 4) * 2]
     far = ((y + 2) % 4) * 2
 
     with scope("attention2"):
-        ga.pass_on(1)
+        each(ga, "pass_on", 1)
     with scope("attention2b"):
-        gw.pass_on(1)
+        each(gw, "pass_on", 1)
     with scope("rows0"):
         for way in (0, 1):
             along(side[way] + c, way, 0, way).wait_recv()
             go(along(side[way] + c, way, 2, way))
+            go(share(side[way] + c, way, 1 + way))
     with scope("attention3"):
-        ga.finish(1)
+        each(ga, "finish", 1)
+    with scope("attention4"):
+        each(gw, "finish", 1)
+        each(gw, "begin", 2)
 
     def widen(f, _):
         WaW[0:PROJ, pl.ds(pl.multiple_of(f * 128, 128), 128)] = Wa[f // 4, f % 4]
@@ -350,72 +373,100 @@
 
     with scope("widen"):
         lax.fori_loop(0, 16, widen, 0)
-    with scope("attention4"):
-        gw.finish(1)
-        gw.begin(2)
 
     def middle(b, size):
         if size >= 8:
-            v = b.reshape(BLK // (2 * size), 2 * size, DK)[:, size - 1 : size, :]
-            return jnp.broadcast_to(v, (BLK // (2 * size), 2 * size, DK)).reshape(BLK, DK)
-        v = b.reshape(BLK // 8, 8, DK)
-        sub = lax.broadcasted_iota(jnp.int32, (BLK // 8, 8, DK), 1)
+            v = b.reshape(BLK // (2 * size), 2 * size, 2 * DK)[:, size - 1 : size, :]
+            return jnp.broadcast_to(v, (BLK // (2 * size), 2 * size, 2 * DK)).reshape(BLK, 2 * DK)
+        v = b.reshape(BLK // 8, 8, 2 * DK)
+        sub = lax.broadcasted_iota(jnp.int32, (BLK // 8, 8, 2 * DK), 1)
         out = None
         for seg in range(8 // (2 * size)):
             at = seg * 2 * size + size - 1
-            here = jnp.broadcast_to(v[:, at : at + 1, :], (BLK // 8, 8, DK))
+            here = jnp.broadcast_to(v[:, at : at + 1, :], (BLK // 8, 8, 2 * DK))
             out = here if out is None else jnp.where(sub >= seg * 2 * size, here, out)
-        return out.reshape(BLK, DK)
-
-    def within(i):
-        rows = pl.ds(pl.multiple_of(i * BLK, BLK), BLK)
-        p = proj[rows, :].astype(BF16)
-        q = p[:, 0:64].astype(F32) * DK**-0.5
-        k = p[:, 64:128].astype(F32)
-        v = p[:, 128:256]
-        pre = dot(p[:, PROJ : PROJ + GR], du_ref[...]) + bias_ref[...]
+        return out.reshape(BLK, 2 * DK)
+
+    def within(pair):
+        spans = [pl.ds(pl.multiple_of((pair + n) * BLK, BLK), BLK) for n in range(2)]
+        p = [proj[rows, :] for rows in spans]
+        qk = [one[:, 0 : 2 * DK].astype(F32) for one in p]
+        left = lax.broadcasted_iota(jnp.int32, (BLK, 2 * DK), 1) < DK
+        q = jnp.where(left, qk[0], pltpu.roll(qk[1], DK, 1)) * DK**-0.5
+        k = jnp.where(left, pltpu.roll(qk[0], DK, 1), qk[1])
+        pre = [dot(one[:, PROJ : PROJ + GR], du2[...]) for one in p]
+        pre = jnp.where(left, pre[0], pre[1]) + bias2[...]
         lg = (jnp.minimum(pre, 0.0) - jnp.log1p(jnp.exp(-jnp.abs(pre)))) / GATE_DIVISOR
-        tri = (level[...] >= 0).astype(F32)
-        b = dot(tri, lg, precision=lax.Precision.HIGHEST)
         lev = level[...]
-        scores = jnp.where(lev == 0, jnp.sum(q * k, axis=1, keepdims=True), 0.0)
-        for n in range(7):
-            e = jnp.exp(-jnp.abs(b - middle(b, 2**n)))
-            s = dot((q * e).astype(BF16), (k * e).astype(BF16), NT)
-            scores = jnp.where(lev == n + 1, s, scores)
-        inner[rows, :] = dot(scores.astype(BF16), v)
-        qe[rows, :] = (q * jnp.exp(b)).astype(BF16)
+        tri = (lev >= 0).astype(BF16)
+        b = jnp.zeros((BLK, 2 * DK), F32)
+        for _ in range(3):
+            top = lg.astype(BF16)
+            b = b + dot(tri, top)
+            lg = lg - top.astype(F32)
+
+        def halves_of(values):
+            values = values.astype(BF16)
+            zero = jnp.zeros_like(values)
+            return [jnp.where(left, values, zero), jnp.where(left, zero, values)]
+
+        scores = None
+        for n in range(8):
+            if n:
+                e = jnp.exp(-jnp.abs(b - middle(b, 2 ** (n - 1))))
+                s = dot(jnp.concatenate(halves_of(q * e), axis=0), (k * e).astype(BF16), NT)
+                scores = [jnp.where(lev == n, s[m * BLK : (m + 1) * BLK], scores[m]) for m in range(2)]
+            else:
+                s = dot(jnp.concatenate(halves_of(q), axis=0), k.astype(BF16), NT)
+                scores = [jnp.where(lev == 0, s[m * BLK : (m + 1) * BLK], 0.0) for m in range(2)]
         last = b[BLK - 1 : BLK, :]
-        shrink[i] = jnp.exp(last)
-        upd[i] = dot(v, (k * jnp.exp(last - b)).astype(BF16), TN)
+        carry = (k * jnp.exp(last - b)).astype(BF16)
+        ends = halves_of(q * jnp.exp(b))
+        fade = jnp.exp(jnp.broadcast_to(last, (8, 2 * DK)))
+        for m in range(2):
+            v = p[m][:, 128:256]
+            inner[spans[m], :] = dot(scores[m].astype(BF16), v)
+            qe[pair + m] = ends[m]
+            both = [dot(v, carry, TN), fade]
+            both = [
+                jnp.where(lax.broadcasted_iota(jnp.int32, one.shape, 1) < DK, *((one, pltpu.roll(one, DK, 1))[:: 1 - 2 * m]))
+                for one in both
+            ]
+            upd[pair + m] = both[0]
+            shrink[pair + m] = both[1]
+            gate[spans[m], :] = silu(p[m][:, 256:384].astype(F32)) * gain_ref[...]
+
+    def arrived(block, slot):
+        for half in range(2):
+            share(block, half, slot).wait_recv()
 
     def project(pair):
         with scope("project"):
             rows = fa[pl.ds(pair, 2)].reshape(2 * ROWS, D)
-            proj[pl.ds(pl.multiple_of(pair * ROWS, 256), 256), 0 : PROJ + GR] = dot(rows, WaW[...], NT)
+            proj[pl.ds(pl.multiple_of(pair * ROWS, 256), 256), 0 : PROJ + GR] = dot(rows, WaW[...], NT).astype(BF16)
         with scope("within"):
             within(pair)
-            within(pair + 1)
-
-    share(t + 1 - 2 * c, 0).wait_recv()
+
+    arrived(t + 1 - 2 * c, 0)
     project(y * 2)
     with scope("rows1"):
         for way in (0, 1):
             along(side[way] + c, 1 - way, 1, way).wait_recv()
-            go(share(side[way] + c, 1 + way))
-    share(side[0] + 1 - c, 1).wait_recv()
+            go(share(side[way] + c, 1 - way, 1 + way))
+    with scope("rows1b"):
+        arrived(side[0] + 1 - c, 1)
     project(side[0])
     with scope("rows2"):
-        share(side[1] + 1 - c, 2).wait_recv()
+        arrived(side[1] + 1 - c, 2)
     project(side[1])
     with scope("attention5"):
-        gw.pass_on(2)
+        each(gw, "pass_on", 2)
     with scope("rows2b"):
         for way in (0, 1):
             along(far + c, way, 2, way).wait_recv()
-        go(share(far + c, 3))
+            go(share(far + c, way, 3))
     with scope("rows3"):
-        share(far + 1 - c, 3).wait_recv()
+        arrived(far + 1 - c, 3)
     project(far)
 
     def home(to):
@@ -425,15 +476,14 @@
             device_id=(r, zl * 4 + x, to * 2 + c), device_id_type=MESH,
         )
 
-    state = jnp.zeros((DV, DK), F32)
+    state = jnp.zeros((DV, 2 * DK), F32)
     with scope("scan"):
         for i in range(8):
             rows = pl.ds(i * BLK, BLK)
-            mixed = inner[rows, :] + dot(qe[rows, :], state.astype(BF16), NT)
-            state = state * shrink[i] + upd[i]
-            normed = mixed * lax.rsqrt(jnp.mean(mixed * mixed, -1, keepdims=True) + HEAD_EPS) * gain_ref[...]
-            gate = proj[rows, 256:384].astype(BF16).astype(F32)
-            gout[rows, :] = (normed * silu(gate)).astype(BF16)
+            mixed = inner[rows, :] + dot(qe[i], state.astype(BF16), NT)
+            state = state * shrink[i, 0:1] + upd[i]
+            spread = jnp.mean(mixed * mixed, -1, keepdims=True)
+            gout[rows, :] = (mixed * lax.rsqrt(spread + HEAD_EPS) * gate[rows, :]).astype(BF16)
             if i % 2:
 
                 @pl.when(y != i // 2)
@@ -445,7 +495,7 @@
                     gin[i // 2] = gout[(i - 1) * BLK : (i + 1) * BLK, :]
 
     with scope("wo"):
-        gw.finish(2)
+        each(gw, "finish", 2)
     settle()
     with scope("home"):
         for step in range(1, 4):
@@ -468,7 +518,7 @@
         return 0
 
     with scope("outp"):
-        halves(out_proj, 1)
+        pieces(out_proj, 1)
     second = joined(1, fa[t], RESIDUAL_SCALE, 1.0, 1)
     xs[...] = second
     xb[c] = second.astype(F32).T.astype(BF16)
@@ -510,30 +560,33 @@
             pltpu.VMEM((2, ROWS, D), F32),
             pltpu.VMEM((3, ROWS, D), F32),
             pltpu.VMEM((8, ROWS, D), BF16),
-            pltpu.VMEM((1024, 512), F32),
+            pltpu.VMEM((1024, 512), BF16),
             pltpu.VMEM((1024, DV), F32),
-            pltpu.VMEM((1024, DK), BF16),
-            pltpu.VMEM((8, DV, DK), F32),
-            pltpu.VMEM((8, 1, DK), F32),
+            pltpu.VMEM((8, BLK, 2 * DK), BF16),
+            pltpu.VMEM((8, DV, 2 * DK), F32),
+            pltpu.VMEM((8, 8, 2 * DK), F32),
+            pltpu.VMEM((1024, DV), F32),
+            pltpu.VMEM((GR, 2 * DK), BF16),
+            pltpu.VMEM((1, 2 * DK), F32),
             pltpu.VMEM((BLK, BLK), jnp.int32),
             pltpu.VMEM((1024, DV), BF16),
             pltpu.VMEM((4, 256, DV), BF16),
             dma((4,)),
             dma((3, 3, 3, 3, 2)),
             dma((3, 3, 3, 3, 2)),
-            dma((2, 3, 2)),
-            dma((2, 3, 2)),
-            dma((3, 3, 2)),
-            dma((3, 3, 2)),
-            dma((12,)),
-            dma((12,)),
+            dma((2, 2, 3, 2)),
+            dma((2, 2, 3, 2)),
+            dma((2, 3, 3, 2)),
+            dma((2, 3, 3, 2)),
+            dma((22,)),
+            dma((22,)),
             dma((3, 2)),
             dma((3, 2)),
             dma((4,)),
             dma((4,)),
         ],
         compiler_params=pltpu.CompilerParams(
-            collective_id=0, has_side_effects=True, vmem_limit_bytes=60 * 1024 * 1024
+            collective_id=0, has_side_effects=True, vmem_limit_bytes=VMEM_LIMIT
         ),
     )(
         stream, gate_weight.T, up_weight.T, down_weight, query_weight.T, key_weight.T, value_weight, outgate_weight,

time: 136 us -> 131 us (0.963)
  Pallas kernels: 134 us -> 129 us
    pallas_call x1, Pallas kernels: 134 us -> 129 us  [on_device(): pl.pallas_call(functools.partial(kernel, stop), out_shape=jax.ShapeDtypeS...]
where the time goes in v3:
time: 131 us
  Pallas kernels  129 us (98%)
  local copies, waits for them, and re-layouts  1.88 us (1%)
    pallas_call x1, Pallas kernels, on_device(): pl.pallas_call(functools.partial(kernel, stop), out_shape=jax.ShapeDtypeS...  129 us

profile of v3, /device:TPU:1, one launch (start us, length us, event | category | flops | bytes accessed | tf_op | source)
XLA Modules:
  0.0 130.8 jit_solution(551452499010425732)
XLA Ops:
  0.0 128.9 %shard_map.136 = bf16[128,2048]{1,0:T(8,128)(2,1)} custom-call(bf16[128,2048]{1,0:T(8,128)(2,1)} %x_ref.1, bf16[352,128]{1,0:T(8,128)(2,1)} %bitcast.8, bf16[352,128]{1,0:T(8,128)(2,1)} %bitcast.9, bf16[352,128]{1,0:T(8,128)(2,1)} %d_ref.1, bf16[64,128]{1,0:T(8,128)(2,1)} %bitcast.10, bf16[64,128]{1,0:T(8,128)(2,1)} %bitcast.11, bf16[128,128]{1,0:T(8,128)(2,1)} %v_ref.1, ...), custom_call_target="tpu_custom_call" | custom-call | tf_op jit(solution)/shard_map/pallas_call | solution.py:545
  128.9 1.9 %copy.16 = bf16[128,2048]{1,0:T(8,128)(2,1)} copy(bf16[128,2048]{1,0:T(8,128)(2,1)} %shard_map.136) | data formatting | bytes 1048576

commit v4 on v3

--- a/solution.py
+++ b/solution.py
@@ -15,6 +15,7 @@
 CHUNKS = ((0, 32, 64), (64, 160, 256), (256, 304, 352))
 SECOND = ((0, HID),)
 PROJ = 384
+DIRECT = True
 VMEM_LIMIT = 60 * 1024 * 1024
 BLK = 128
 RESIDUAL_SCALE = 2.0**0.5
@@ -50,57 +51,65 @@
 
 
 class Gather:
-    def __init__(self, order, at, rows, send, recv, pending):
+    def __init__(self, order, at, rows, send, recv, direct=()):
         self.order, self.at, self.rows = order, at, rows
-        self.send, self.recv, self.pending = send, recv, pending
+        self.send, self.recv, self.direct = send, recv, direct
         r, zl, x, y, c = place()
         self.pos = {"x": x, "y": y, "z": zl}
 
-    def region(self, phase, shift, half):
-        lo, mid, hi = self.rows
-        lo, hi = ((lo, mid), (mid, hi))[half]
+    def region(self, phase, along, lo, hi):
         idx = {}
         for k, dim in enumerate(self.order):
             if k < phase:
                 idx[dim] = slice(None)
             elif k == phase:
-                idx[dim] = (self.pos[dim] + shift) % 4
+                idx[dim] = along
             else:
                 idx[dim] = self.pos[dim]
         return self.at(idx, pl.ds(lo, hi - lo))
 
-    def copy(self, phase, shift, half, stage, way):
-        region = self.region(phase, shift, half)
+    def copy(self, phase, region, late, step):
         return pltpu.make_async_remote_copy(
             src_ref=region,
             dst_ref=region,
-            send_sem=self.send(phase, stage, way),
-            recv_sem=self.recv(phase, stage, way),
-            device_id=neighbour(self.order[phase], 1 if way == 0 else -1),
+            send_sem=self.send(phase),
+            recv_sem=self.recv(phase, late),
+            device_id=neighbour(self.order[phase], step),
             device_id_type=MESH,
         )
 
-    def go(self, *args):
-        cp = self.copy(*args)
-        cp.start()
-        self.pending.append(cp)
+    def go(self, phase, shift, half, late, step):
+        lo, mid, hi = self.rows
+        lo, hi = ((lo, mid), (mid, hi))[half]
+        self.copy(phase, self.region(phase, (self.pos[self.order[phase]] + shift) % 4, lo, hi), late, step).start()
+
+    def whole(self, phase, count, late, lo, hi):
+        return self.copy(phase, self.region(phase, pl.ds(0, count), lo, hi), late, 1)
 
     def begin(self, phase):
-        for stage in (0, 1):
+        for late in (0, 1):
             for way in (0, 1):
-                self.go(phase, 0, way ^ stage, stage, way)
+                self.go(phase, 0, way ^ late, late, 1 - 2 * way)
+        if phase in self.direct:
+            for way in (0, 1):
+                self.go(phase, 0, way, 1, 2 - 4 * way)
+
+    def first_halves(self, phase):
+        self.whole(phase, 1, 0, self.rows[0], self.rows[2]).wait_recv()
 
     def pass_on(self, phase):
-        for way in (0, 1):
-            self.copy(phase, 3 - 2 * way, way, 0, way).wait_recv()
-        for way in (0, 1):
-            self.go(phase, 3 - 2 * way, way, 2, way)
+        if phase not in self.direct:
+            self.first_halves(phase)
+            for way in (0, 1):
+                self.go(phase, 3 - 2 * way, way, 1, 1 - 2 * way)
 
     def finish(self, phase):
-        for way in (0, 1):
-            self.copy(phase, 3 - 2 * way, 1 - way, 1, way).wait_recv()
-        for way in (0, 1):
-            self.copy(phase, 2, way, 2, way).wait_recv()
+        if phase in self.direct:
+            self.first_halves(phase)
+        self.whole(phase, 2, 1, self.rows[0], self.rows[2]).wait_recv()
+
+    def sent(self, phase, lo, hi):
+        self.whole(phase, 3, 0, lo, hi).wait_send()
 
 
 def layer_norm(values, norm_scale):
@@ -113,15 +122,19 @@
 scope = jax.named_scope
 
 
+def column_block(j):
+    return pl.ds(j * 256 if isinstance(j, int) else pl.multiple_of(j * 256, 256), 256)
+
+
 def silu(v):
     return v / (1.0 + jnp.exp(-v))
 
 
 def kernel(
     stop,
-    x_ref, g_ref, u_ref, d_ref, q_ref, k_ref, v_ref, og_ref, dd_ref, du_ref, bias_ref, gain_ref, wo_ref, norm_ref,
+    x_hbm, g_ref, u_ref, d_ref, q_hbm, k_hbm, v_hbm, og_hbm, dd_hbm, du_ref, bias_ref, gain_ref, wo_ref, norm_ref,
     out_ref,
-    W, Wa, Wo, WaW, xa, xb, xs, hidT, hid, acc, part, fa, proj, inner, qe, upd, shrink, gate, du2, bias2, level,
+    x_ref, q_ref, k_ref, v_ref, og_ref, W, Wa, Wo, WaW, xa, xb, xs, hidT, hid, acc, part, fa, proj, inner, qe, upd, shrink, gate, du2, bias2, level,
     gout, gin,
     lsem, fsend, frecv, asend, arecv, osend, orecv, csend, crecv, ysend, yrecv, hsend, hrecv,
 ):
@@ -129,18 +142,26 @@
     t = y * 2 + c
     barrier = pltpu.get_barrier_semaphore()
     for dim in "xyz":
-        for step in (1, -1):
+        for step in (1, -1, 2, -2) if dim == "z" else (1, -1, 2):
             pl.semaphore_signal(barrier, 1, device_id=neighbour(dim, step), device_id_type=MESH)
     pl.semaphore_signal(barrier, 1, device_id=neighbour("c", 1), device_id_type=MESH)
-    pl.semaphore_signal(barrier, 1, device_id=neighbour("y", 2), device_id_type=MESH)
     own = []
     for w, ref in enumerate((g_ref, u_ref, d_ref)):
         own.append(pltpu.make_async_copy(ref, W.at[w, y, zl, x], lsem.at[w]))
-    own.append(pltpu.make_async_copy(wo_ref, Wo.at[y, zl, x], lsem.at[3]))
-    for cp in own:
+    later = [pltpu.make_async_copy(wo_ref, Wo.at[y, zl, x], lsem.at[3])]
+    for src, dst in (
+        (q_hbm, q_ref),
+        (k_hbm, k_ref),
+        (v_hbm, v_ref),
+        (og_hbm, og_ref),
+        (dd_hbm, WaW.at[PROJ : PROJ + GR]),
+        (x_hbm, x_ref),
+    ):
+        later.append(pltpu.make_async_copy(src, dst, lsem.at[3 + len(later)]))
+    for cp in own + later:
         cp.start()
     with scope("barrier"):
-        pl.semaphore_wait(barrier, 8)
+        pl.semaphore_wait(barrier, 11)
         for cp in own:
             cp.wait()
 
@@ -168,25 +189,23 @@
             orders[w],
             lambda idx, rows: W.at[w, idx["y"], idx["z"], idx["x"], rows],
             CHUNKS[ch],
-            lambda ph, st, way: fsend.at[ch, w, ph, st, way],
-            lambda ph, st, way: frecv.at[ch, w, ph, st, way],
-            pending,
+            lambda ph: fsend.at[w, ph],
+            lambda ph, late: frecv.at[ch, w, ph, late],
+            (0,) if ch == 0 and DIRECT else (),
         )
 
     ffn = [[ffn_gather(ch, w) for w in range(3)] for ch in range(3)]
     ga = [
         Gather(
             order, lambda idx, rows: Wa.at[idx["z"], idx["x"], rows], span,
-            lambda ph, st, way, n=n: asend.at[n, ph, st, way], lambda ph, st, way, n=n: arecv.at[n, ph, st, way],
-            pending,
+            lambda ph, n=n: asend.at[n, ph], lambda ph, late, n=n: arecv.at[n, ph, late],
         )
         for n, (order, span) in enumerate(((("x", "z"), (0, 96, 192)), (("z", "x"), (192, 288, 384))))
     ]
     gw = [
         Gather(
             order, lambda idx, rows: Wo.at[idx["y"], idx["z"], idx["x"], rows], span,
-            lambda ph, st, way, n=n: osend.at[n, ph, st, way], lambda ph, st, way, n=n: orecv.at[n, ph, st, way],
-            pending,
+            lambda ph, n=n: osend.at[n, ph], lambda ph, late, n=n: orecv.at[n, ph, late],
         )
         for n, (order, span) in enumerate(((("y", "x", "z"), (0, 32, 64)), (("y", "z", "x"), (64, 96, 128))))
     ]
@@ -211,13 +230,15 @@
         size = hi - lo
 
         def body(yy, _):
-            gate, up = (
-                dot(
-                    jnp.concatenate([W[w, yy, f // 4, f % 4, lo:hi, :] for f in range(16)], axis=1),
-                    jnp.concatenate([rows[0], rows[1]], axis=1),
-                )
-                for w in (0, 1)
-            )
+            both = [
+                jnp.concatenate([W[w, yy, f // 4, f % 4, lo:hi, :] for f in range(16)], axis=1) for w in (0, 1)
+            ]
+            if size < 128:
+                both = [jnp.concatenate(both, axis=0)]
+            wide = jnp.concatenate([rows[0], rows[1]], axis=1)
+            products = [dot(one, wide) for one in both]
+            gate = products[0][:size]
+            up = products[-1][-size:]
             hidT[pl.ds(pl.multiple_of(yy * size, 16), size), :] = silu(gate) * up
             return 0
 
@@ -227,48 +248,67 @@
     def down(lo, hi, slot):
         size = hi - lo
 
-        def body(j, _):
-            weights = jnp.concatenate(
+        def weights(j):
+            return jnp.concatenate(
                 [
                     jnp.concatenate([W[2, yy, j // 2, (j % 2) * 2 + i, lo:hi, :] for i in range(2)], axis=1)
                     for yy in range(4)
                 ],
                 axis=0,
             )
-            cols = pl.ds(pl.multiple_of(j * 256, 256), 256)
-            term = dot(hid[:, : 4 * size], weights)
+
+        def body(j, _):
+            term = dot(hid[:, : 4 * size], weights(j))
             for half in range(2):
                 piece = term[half * ROWS : (half + 1) * ROWS]
                 if lo:
-                    acc[half, :, cols] += piece
+                    acc[half, :, column_block(j)] += piece
                 else:
-                    acc[half, :, cols] = piece
+                    acc[half, :, column_block(j)] = piece
             return 0
 
+        def one(j, who):
+            term = dot(hid[rows_of(who), : 4 * size], weights(j))
+            if lo:
+                acc[who, :, column_block(j)] += term
+            else:
+                acc[who, :, column_block(j)] = term
+
         if hi == HID:
-            pieces(body, slot)
+            pieces(one, slot)
         else:
             lax.fori_loop(0, 8, body, 0, unroll=2)
 
+    def rows_of(who):
+        return pl.ds(pl.multiple_of(who * ROWS, ROWS), ROWS)
+
     def give(slot, piece):
         cols = pl.ds(piece * 512, 512)
-        return across(acc.at[1 - c, :, cols], part.at[slot, :, cols], 2 + 4 * slot + piece)
-
-    def pieces(body, slot):
+        return across(acc.at[1 - c, :, cols], part.at[slot, :, cols], 2 + slot)
+
+    def given(slot):
+        return across(acc.at[1 - c], part.at[slot], 2 + slot)
+
+    def pieces(one, slot):
         for piece in range(4):
-            lax.fori_loop(piece * 2, piece * 2 + 2, body, 0, unroll=True)
-            go(give(slot, piece))
+            for j in range(piece * 2, piece * 2 + 2):
+                one(j, 1 - c)
+            give(slot, piece).start()
+        pending.append(given(slot))
+        for j in range(8):
+            one(j, c)
 
     def joined(slot, residual, scale, branch, norm):
         with scope(f"swap_{slot}"):
-            for piece in range(4):
-                give(slot, piece).wait_recv()
+            given(slot).wait_recv()
         with scope(f"norm_{slot}"):
             total = acc[c] + part[slot]
             return layer_norm(scale * residual.astype(F32) + branch * total, norm_ref[norm : norm + 1, :])
 
     for ch in range(3):
         begin(ch, 0)
+    for cp in later:
+        cp.wait()
     Wa[zl, x, 0:64, :] = q_ref[...]
     Wa[zl, x, 64:128, :] = k_ref[...]
     Wa[zl, x, 128:256, :] = v_ref[...].astype(F32).T.astype(BF16)
@@ -301,7 +341,6 @@
     for k in range(7):
         bits = bits + (differ >= 2**k).astype(jnp.int32)
     level[...] = jnp.where(rowi >= coli, bits, -1)
-    WaW[PROJ : PROJ + GR, :] = dd_ref[...]
 
     def ffn_compute(span, rows, slot):
         with scope(f"hidden{span[0]}"):
@@ -345,10 +384,12 @@
 
     def share(block, half, slot):
         ref = fa.at[block, half_rows[half]]
-        return across(ref, ref, 14 + 2 * slot + half)
-
-    go(share(t, 0, 0))
-    go(share(t, 1, 0))
+        across(ref, ref, 5 + slot).start()
+
+    def shared(block, slot):
+        return across(fa.at[block], fa.at[block], 5 + slot)
+
+    go(shared(t, 0))
     side = [((y + 3) % 4) * 2, ((y + 1) % 4) * 2]
     far = ((y + 2) % 4) * 2
 
@@ -360,7 +401,7 @@
         for way in (0, 1):
             along(side[way] + c, way, 0, way).wait_recv()
             go(along(side[way] + c, way, 2, way))
-            go(share(side[way] + c, way, 1 + way))
+            share(side[way] + c, way, 1 + way)
     with scope("attention3"):
         each(ga, "finish", 1)
     with scope("attention4"):
@@ -437,8 +478,7 @@
             gate[spans[m], :] = silu(p[m][:, 256:384].astype(F32)) * gain_ref[...]
 
     def arrived(block, slot):
-        for half in range(2):
-            share(block, half, slot).wait_recv()
+        shared(block, slot).wait_recv()
 
     def project(pair):
         with scope("project"):
@@ -452,7 +492,8 @@
     with scope("rows1"):
         for way in (0, 1):
             along(side[way] + c, 1 - way, 1, way).wait_recv()
-            go(share(side[way] + c, 1 - way, 1 + way))
+            share(side[way] + c, 1 - way, 1 + way)
+            pending.append(shared(side[way] + c, 1 + way))
     with scope("rows1b"):
         arrived(side[0] + 1 - c, 1)
     project(side[0])
@@ -464,7 +505,8 @@
     with scope("rows2b"):
         for way in (0, 1):
             along(far + c, way, 2, way).wait_recv()
-            go(share(far + c, way, 3))
+            share(far + c, way, 3)
+        pending.append(shared(far + c, 3))
     with scope("rows3"):
         arrived(far + 1 - c, 3)
     project(far)
@@ -506,25 +548,32 @@
                 device_id=(r, zl * 4 + x, source * 2 + c), device_id_type=MESH,
             ).wait()
 
-    def out_proj(j, _):
+    def out_proj(j, who):
         weights = jnp.concatenate(
             [jnp.concatenate([Wo[yy, j // 2, (j % 2) * 2 + i] for i in range(2)], axis=1) for yy in range(4)],
             axis=0,
         )
-        cols = pl.ds(pl.multiple_of(j * 256, 256), 256)
-        term = dot(jnp.concatenate([gin[yy] for yy in range(4)], axis=1), weights)
-        acc[0, :, cols] = term[:ROWS]
-        acc[1, :, cols] = term[ROWS:]
-        return 0
+        rows = jnp.concatenate([gin[yy, rows_of(who)] for yy in range(4)], axis=1)
+        acc[who, :, column_block(j)] = dot(rows, weights)
 
     with scope("outp"):
         pieces(out_proj, 1)
     second = joined(1, fa[t], RESIDUAL_SCALE, 1.0, 1)
     xs[...] = second
-    xb[c] = second.astype(F32).T.astype(BF16)
-    go(across(xb.at[c], xb.at[c], 1))
+
+
+    def hand(piece):
+        ref = xb.at[c, pl.ds(piece * 1024, 1024)]
+        return across(ref, ref, 1)
+
+    for piece in range(2):
+        span = slice(piece * 1024, (piece + 1) * 1024)
+        xb[c, span] = second[:, span].astype(F32).T.astype(BF16)
+        hand(piece).start()
+    both = across(xb.at[c], xb.at[c], 1)
+    pending.append(both)
     with scope("swapx"):
-        across(xb.at[1 - c], xb.at[1 - c], 1).wait_recv()
+        both.wait_recv()
     settle()
     for span in SECOND:
         ffn_compute(span, xb, 2)
@@ -534,20 +583,30 @@
     if stop == 2:
         out_ref[...] = xs[...]
     settle()
+    for phase in range(3):
+        for g in ffn[0]:
+            g.sent(phase, 0, HID)
+        for g in gw + (ga if phase < 2 else []):
+            g.sent(phase, g.rows[0], g.rows[2])
 
 
 def on_device(
     stop, stream, gate_weight, up_weight, down_weight, query_weight, key_weight, value_weight, outgate_weight,
     decay_down, decay_up, decay_bias, head_gain, out_weight, norm_gain,
 ):
-    vmem = pl.BlockSpec(memory_space=pltpu.VMEM)
+    vmem, hbm = (pl.BlockSpec(memory_space=space) for space in (pltpu.VMEM, pltpu.HBM))
     dma = pltpu.SemaphoreType.DMA
     return pl.pallas_call(
         functools.partial(kernel, stop),
         out_shape=jax.ShapeDtypeStruct((ROWS, D), BF16),
-        in_specs=[vmem] * 14,
+        in_specs=[hbm] * 9 + [vmem] * 3 + [hbm, vmem],
         out_specs=vmem,
         scratch_shapes=[
+            pltpu.VMEM((ROWS, D), BF16),
+            pltpu.VMEM((DK, 128), BF16),
+            pltpu.VMEM((DK, 128), BF16),
+            pltpu.VMEM((128, DV), BF16),
+            pltpu.VMEM((128, DV), BF16),
             pltpu.VMEM((3, 4, 4, 4, HID, 128), BF16),
             pltpu.VMEM((4, 4, PROJ, 128), BF16),
             pltpu.VMEM((4, 4, 4, 128, 128), BF16),
@@ -571,15 +630,15 @@
             pltpu.VMEM((BLK, BLK), jnp.int32),
             pltpu.VMEM((1024, DV), BF16),
             pltpu.VMEM((4, 256, DV), BF16),
-            dma((4,)),
-            dma((3, 3, 3, 3, 2)),
-            dma((3, 3, 3, 3, 2)),
-            dma((2, 2, 3, 2)),
-            dma((2, 2, 3, 2)),
-            dma((2, 3, 3, 2)),
-            dma((2, 3, 3, 2)),
-            dma((22,)),
-            dma((22,)),
+            dma((10,)),
+            dma((3, 3)),
+            dma((3, 3, 3, 2)),
+            dma((2, 2)),
+            dma((2, 2, 2)),
+            dma((2, 3)),
+            dma((2, 3, 2)),
+            dma((9,)),
+            dma((9,)),
             dma((3, 2)),
             dma((3, 2)),
             dma((4,)),

time: 131 us -> 125 us (0.954)
  Pallas kernels: 129 us -> 123 us
    pallas_call x1, Pallas kernels: 129 us -> 123 us  [on_device(): pl.pallas_call(functools.partial(kernel, stop), out_shape=jax.ShapeDtypeS...]
where the time goes in v4:
time: 125 us
  Pallas kernels  123 us (98%)
  local copies, waits for them, and re-layouts  1.88 us (2%)
    pallas_call x1, Pallas kernels, on_device(): pl.pallas_call(functools.partial(kernel, stop), out_shape=jax.ShapeDtypeS...  123 us

profile of v4, /device:TPU:1, one launch (start us, length us, event | category | flops | bytes accessed | tf_op | source)
XLA Modules:
  0.0 125.0 jit_solution(10320158250351142649)
XLA Ops:
  0.0 123.1 %shard_map.136 = bf16[128,2048]{1,0:T(8,128)(2,1)} custom-call(bf16[128,2048]{1,0:T(8,128)(2,1)} %x_hbm.1, bf16[352,128]{1,0:T(8,128)(2,1)} %bitcast.8, bf16[352,128]{1,0:T(8,128)(2,1)} %bitcast.9, bf16[352,128]{1,0:T(8,128)(2,1)} %d_ref.1, bf16[64,128]{1,0:T(8,128)(2,1)} %bitcast.10, bf16[64,128]{1,0:T(8,128)(2,1)} %bitcast.11, bf16[128,128]{1,0:T(8,128)(2,1)} %v_hbm.1, ...), custom_call_target="tpu_custom_call" | custom-call | tf_op jit(solution)/shard_map/pallas_call | solution.py:599
  123.1 1.9 %copy.16 = bf16[128,2048]{1,0:T(8,128)(2,1)} copy(bf16[128,2048]{1,0:T(8,128)(2,1)} %shard_map.136) | data formatting | bytes 1048576

commit v5 on v4

--- a/solution.py
+++ b/solution.py
@@ -134,7 +134,7 @@
     stop,
     x_hbm, g_ref, u_ref, d_ref, q_hbm, k_hbm, v_hbm, og_hbm, dd_hbm, du_ref, bias_ref, gain_ref, wo_ref, norm_ref,
     out_ref,
-    x_ref, q_ref, k_ref, v_ref, og_ref, W, Wa, Wo, WaW, xa, xb, xs, hidT, hid, acc, part, fa, proj, inner, qe, upd, shrink, gate, du2, bias2, level,
+    x_ref, q_ref, k_ref, v_ref, og_ref, W, Wa, Wo, WaW, xa, xb, xs, hidT, hid, acc, part, fa, proj, inner, qe, upd, shrink, states, gate, du2, bias2, level,
     gout, gin,
     lsem, fsend, frecv, asend, arecv, osend, orecv, csend, crecv, ysend, yrecv, hsend, hrecv,
 ):
@@ -144,11 +144,12 @@
     for dim in "xyz":
         for step in (1, -1, 2, -2) if dim == "z" else (1, -1, 2):
             pl.semaphore_signal(barrier, 1, device_id=neighbour(dim, step), device_id_type=MESH)
-    pl.semaphore_signal(barrier, 1, device_id=neighbour("c", 1), device_id_type=MESH)
+    for step in range(4):
+        pl.semaphore_signal(barrier, 1, device_id=(r, zl * 4 + x, ((y + step) % 4) * 2 + 1 - c), device_id_type=MESH)
     own = []
     for w, ref in enumerate((g_ref, u_ref, d_ref)):
         own.append(pltpu.make_async_copy(ref, W.at[w, y, zl, x], lsem.at[w]))
-    later = [pltpu.make_async_copy(wo_ref, Wo.at[y, zl, x], lsem.at[3])]
+    later = [pltpu.make_async_copy(wo_ref, Wo.at[c, y, zl, x], lsem.at[3])]
     for src, dst in (
         (q_hbm, q_ref),
         (k_hbm, k_ref),
@@ -161,7 +162,7 @@
     for cp in own + later:
         cp.start()
     with scope("barrier"):
-        pl.semaphore_wait(barrier, 11)
+        pl.semaphore_wait(barrier, 14)
         for cp in own:
             cp.wait()
 
@@ -204,7 +205,7 @@
     ]
     gw = [
         Gather(
-            order, lambda idx, rows: Wo.at[idx["y"], idx["z"], idx["x"], rows], span,
+            order, lambda idx, rows: Wo.at[c, idx["y"], idx["z"], idx["x"], rows], span,
             lambda ph, n=n: osend.at[n, ph], lambda ph, late, n=n: orecv.at[n, ph, late],
         )
         for n, (order, span) in enumerate(((("y", "x", "z"), (0, 32, 64)), (("y", "z", "x"), (64, 96, 128))))
@@ -397,6 +398,9 @@
         each(ga, "pass_on", 1)
     with scope("attention2b"):
         each(gw, "pass_on", 1)
+    with scope("attention4"):
+        each(gw, "finish", 1)
+        each(gw, "begin", 2)
     with scope("rows0"):
         for way in (0, 1):
             along(side[way] + c, way, 0, way).wait_recv()
@@ -404,9 +408,6 @@
             share(side[way] + c, way, 1 + way)
     with scope("attention3"):
         each(ga, "finish", 1)
-    with scope("attention4"):
-        each(gw, "finish", 1)
-        each(gw, "begin", 2)
 
     def widen(f, _):
         WaW[0:PROJ, pl.ds(pl.multiple_of(f * 128, 128), 128)] = Wa[f // 4, f % 4]
@@ -480,6 +481,9 @@
     def arrived(block, slot):
         shared(block, slot).wait_recv()
 
+    def project_one(block):
+        proj[rows_of(block), 0 : PROJ + GR] = dot(fa[block], WaW[...], NT).astype(BF16)
+
     def project(pair):
         with scope("project"):
             rows = fa[pl.ds(pair, 2)].reshape(2 * ROWS, D)
@@ -494,71 +498,79 @@
             along(side[way] + c, 1 - way, 1, way).wait_recv()
             share(side[way] + c, 1 - way, 1 + way)
             pending.append(shared(side[way] + c, 1 + way))
+    with scope("attention5"):
+        each(gw, "pass_on", 2)
     with scope("rows1b"):
         arrived(side[0] + 1 - c, 1)
     project(side[0])
     with scope("rows2"):
         arrived(side[1] + 1 - c, 2)
     project(side[1])
-    with scope("attention5"):
-        each(gw, "pass_on", 2)
     with scope("rows2b"):
         for way in (0, 1):
             along(far + c, way, 2, way).wait_recv()
             share(far + c, way, 3)
         pending.append(shared(far + c, 3))
+    project_one(far + c)
     with scope("rows3"):
         arrived(far + 1 - c, 3)
-    project(far)
-
-    def home(to):
+    project_one(far + 1 - c)
+    with scope("wo"):
+        each(gw, "finish", 2)
+    go(across(Wo.at[c], Wo.at[c], 9))
+    with scope("within"):
+        within(far)
+
+    def home(step, other):
+        to = (y + step) % 4
+        core = c + other - 2 * c * other
         return pltpu.make_async_remote_copy(
-            src_ref=gout.at[pl.ds(to * 256, 256)], dst_ref=gin.at[y],
-            send_sem=hsend.at[to], recv_sem=hrecv.at[y],
-            device_id=(r, zl * 4 + x, to * 2 + c), device_id_type=MESH,
+            src_ref=gout.at[rows_of(to * 2 + core)], dst_ref=gin.at[t],
+            send_sem=hsend.at[step, other], recv_sem=hrecv.at[step, other],
+            device_id=(r, zl * 4 + x, to * 2 + core), device_id_type=MESH,
         )
 
     state = jnp.zeros((DV, 2 * DK), F32)
     with scope("scan"):
         for i in range(8):
-            rows = pl.ds(i * BLK, BLK)
-            mixed = inner[rows, :] + dot(qe[i], state.astype(BF16), NT)
+            states[i] = state.astype(BF16)
             state = state * shrink[i, 0:1] + upd[i]
-            spread = jnp.mean(mixed * mixed, -1, keepdims=True)
-            gout[rows, :] = (mixed * lax.rsqrt(spread + HEAD_EPS) * gate[rows, :]).astype(BF16)
-            if i % 2:
-
-                @pl.when(y != i // 2)
-                def _():
-                    home(i // 2).start()
-
-                @pl.when(y == i // 2)
-                def _():
-                    gin[i // 2] = gout[(i - 1) * BLK : (i + 1) * BLK, :]
-
-    with scope("wo"):
-        each(gw, "finish", 2)
+        for step in (2, 1, 3, 0):
+            to = (y + step) % 4
+            for m in range(2):
+                i = to * 2 + m
+                rows = pl.ds(pl.multiple_of(i * BLK, BLK), BLK)
+                mixed = inner[rows, :] + dot(qe[i], states[i], NT)
+                spread = jnp.mean(mixed * mixed, -1, keepdims=True)
+                done = (mixed * lax.rsqrt(spread + HEAD_EPS) * gate[rows, :]).astype(BF16)
+                gout[rows, :] = done
+            for other in range(2):
+                if step or other:
+                    go(home(step, other))
+        gin[t] = gout[rows_of(t), :]
+
+    with scope("home"):
+        for step in (0, 1, 3, 2):
+            for other in range(2):
+                if step or other:
+                    home(step, other).wait_recv()
+    with scope("wo2"):
+        across(Wo.at[1 - c], Wo.at[1 - c], 9).wait_recv()
+
     settle()
-    with scope("home"):
-        for step in range(1, 4):
-            source = (y + step) % 4
-            pltpu.make_async_remote_copy(
-                src_ref=gout.at[pl.ds(0, 256)], dst_ref=gin.at[source],
-                send_sem=hsend.at[source], recv_sem=hrecv.at[source],
-                device_id=(r, zl * 4 + x, source * 2 + c), device_id_type=MESH,
-            ).wait()
-
-    def out_proj(j, who):
-        weights = jnp.concatenate(
-            [jnp.concatenate([Wo[yy, j // 2, (j % 2) * 2 + i] for i in range(2)], axis=1) for yy in range(4)],
-            axis=0,
-        )
-        rows = jnp.concatenate([gin[yy, rows_of(who)] for yy in range(4)], axis=1)
-        acc[who, :, column_block(j)] = dot(rows, weights)
-
     with scope("outp"):
-        pieces(out_proj, 1)
-    second = joined(1, fa[t], RESIDUAL_SCALE, 1.0, 1)
+        rows = jnp.concatenate([gin[head] for head in range(8)], axis=1)
+        for j in range(8):
+            weights = jnp.concatenate(
+                [
+                    jnp.concatenate([Wo[head % 2, head // 2, j // 2, (j % 2) * 2 + i] for i in range(2)], axis=1)
+                    for head in range(8)
+                ],
+                axis=0,
+            )
+            acc[c, :, column_block(j)] = dot(rows, weights)
+    with scope("norm_1"):
+        second = layer_norm(RESIDUAL_SCALE * fa[t].astype(F32) + acc[c], norm_ref[1:2, :])
     xs[...] = second
 
 
@@ -609,7 +621,7 @@
             pltpu.VMEM((128, DV), BF16),
             pltpu.VMEM((3, 4, 4, 4, HID, 128), BF16),
             pltpu.VMEM((4, 4, PROJ, 128), BF16),
-            pltpu.VMEM((4, 4, 4, 128, 128), BF16),
+            pltpu.VMEM((2, 4, 4, 4, 128, 128), BF16),
             pltpu.VMEM((PROJ + GR, D), BF16),
             pltpu.VMEM((2, D, ROWS), BF16),
             pltpu.VMEM((2, D, ROWS), BF16),
@@ -624,12 +636,13 @@
             pltpu.VMEM((8, BLK, 2 * DK), BF16),
             pltpu.VMEM((8, DV, 2 * DK), F32),
             pltpu.VMEM((8, 8, 2 * DK), F32),
+            pltpu.VMEM((8, DV, 2 * DK), BF16),
             pltpu.VMEM((1024, DV), F32),
             pltpu.VMEM((GR, 2 * DK), BF16),
             pltpu.VMEM((1, 2 * DK), F32),
             pltpu.VMEM((BLK, BLK), jnp.int32),
             pltpu.VMEM((1024, DV), BF16),
-            pltpu.VMEM((4, 256, DV), BF16),
+            pltpu.VMEM((8, ROWS, DV), BF16),
             dma((10,)),
             dma((3, 3)),
             dma((3, 3, 3, 2)),
@@ -637,12 +650,12 @@
             dma((2, 2, 2)),
             dma((2, 3)),
             dma((2, 3, 2)),
-            dma((9,)),
-            dma((9,)),
+            dma((10,)),
+            dma((10,)),
             dma((3, 2)),
             dma((3, 2)),
-            dma((4,)),
-            dma((4,)),
+            dma((4, 2)),
+            dma((4, 2)),
         ],
         compiler_params=pltpu.CompilerParams(
             collective_id=0, has_side_effects=True, vmem_limit_bytes=VMEM_LIMIT

time: 125 us -> 124 us (level)
    pallas_call x1, Pallas kernels: 123 us -> 122 us  [on_device(): pl.pallas_call(functools.partial(kernel, stop), out_shape=jax.ShapeDtypeS...]
where the time goes in v5:
time: 124 us
  Pallas kernels  122 us (98%)
  local copies, waits for them, and re-layouts  1.88 us (2%)
    pallas_call x1, Pallas kernels, on_device(): pl.pallas_call(functools.partial(kernel, stop), out_shape=jax.ShapeDtypeS...  122 us

profile of v5, /device:TPU:1, one launch (start us, length us, event | category | flops | bytes accessed | tf_op | source)
XLA Modules:
  0.0 123.6 jit_solution(10596548800570924798)
XLA Ops:
  0.0 121.7 %shard_map.136 = bf16[128,2048]{1,0:T(8,128)(2,1)} custom-call(bf16[128,2048]{1,0:T(8,128)(2,1)} %x_hbm.1, bf16[352,128]{1,0:T(8,128)(2,1)} %bitcast.8, bf16[352,128]{1,0:T(8,128)(2,1)} %bitcast.9, bf16[352,128]{1,0:T(8,128)(2,1)} %d_ref.1, bf16[64,128]{1,0:T(8,128)(2,1)} %bitcast.10, bf16[64,128]{1,0:T(8,128)(2,1)} %bitcast.11, bf16[128,128]{1,0:T(8,128)(2,1)} %v_hbm.1, ...), custom_call_target="tpu_custom_call" | custom-call | tf_op jit(solution)/shard_map/pallas_call | solution.py:611
  121.7 1.9 %copy.16 = bf16[128,2048]{1,0:T(8,128)(2,1)} copy(bf16[128,2048]{1,0:T(8,128)(2,1)} %shard_map.136) | data formatting | bytes 1048576

commit v6 on v5

--- a/solution.py
+++ b/solution.py
@@ -12,7 +12,7 @@
 D, DK, DV, GR = 2048, 64, 128, 32
 ROWS = 128
 HID = 352
-CHUNKS = ((0, 32, 64), (64, 160, 256), (256, 304, 352))
+CHUNKS = ((0, 32, 64), (64, 176, 288), (288, 320, 352))
 SECOND = ((0, HID),)
 PROJ = 384
 DIRECT = True
@@ -192,7 +192,7 @@
             CHUNKS[ch],
             lambda ph: fsend.at[w, ph],
             lambda ph, late: frecv.at[ch, w, ph, late],
-            (0,) if ch == 0 and DIRECT else (),
+            (0, 1) if ch == 0 and DIRECT else (),
         )
 
     ffn = [[ffn_gather(ch, w) for w in range(3)] for ch in range(3)]
@@ -360,14 +360,14 @@
     pass_on(1, 2)
     begin(2, 2)
     finish(1)
-    ffn_compute((64, 256), xa, 0)
+    ffn_compute((64, 288), xa, 0)
     pass_on(2, 2)
     each(ga, "finish", 0)
     each(ga, "begin", 1)
     each(gw, "finish", 0)
     each(gw, "begin", 1)
     finish(2)
-    ffn_compute((256, HID), xa, 0)
+    ffn_compute((288, HID), xa, 0)
     fa[t] = joined(0, x_ref[...], RESIDUAL_SCALE, BRANCH_SCALE, 0)
 
     half_rows = (pl.ds(0, ROWS // 2), pl.ds(ROWS // 2, ROWS // 2))
@@ -575,11 +575,11 @@
 
 
     def hand(piece):
-        ref = xb.at[c, pl.ds(piece * 1024, 1024)]
+        ref = xb.at[c, pl.ds(piece * 512, 512)]
         return across(ref, ref, 1)
 
-    for piece in range(2):
-        span = slice(piece * 1024, (piece + 1) * 1024)
+    for piece in range(4):
+        span = slice(piece * 512, (piece + 1) * 512)
         xb[c, span] = second[:, span].astype(F32).T.astype(BF16)
         hand(piece).start()
     both = across(xb.at[c], xb.at[c], 1)

time: 124 us -> 123 us (level)
  no operation moved by 1% of the time
where the time goes in v6:
time: 123 us
  Pallas kernels  121 us (98%)
  local copies, waits for them, and re-layouts  1.88 us (2%)
    pallas_call x1, Pallas kernels, on_device(): pl.pallas_call(functools.partial(kernel, stop), out_shape=jax.ShapeDtypeS...  121 us

profile of v6, /device:TPU:1, one launch (start us, length us, event | category | flops | bytes accessed | tf_op | source)
XLA Modules:
  0.0 123.3 jit_solution(5228920290916542746)
XLA Ops:
  0.0 121.4 %shard_map.136 = bf16[128,2048]{1,0:T(8,128)(2,1)} custom-call(bf16[128,2048]{1,0:T(8,128)(2,1)} %x_hbm.1, bf16[352,128]{1,0:T(8,128)(2,1)} %bitcast.8, bf16[352,128]{1,0:T(8,128)(2,1)} %bitcast.9, bf16[352,128]{1,0:T(8,128)(2,1)} %d_ref.1, bf16[64,128]{1,0:T(8,128)(2,1)} %bitcast.10, bf16[64,128]{1,0:T(8,128)(2,1)} %bitcast.11, bf16[128,128]{1,0:T(8,128)(2,1)} %v_hbm.1, ...), custom_call_target="tpu_custom_call" | custom-call | tf_op jit(solution)/shard_map/pallas_call | solution.py:611
  121.4 1.9 %copy.16 = bf16[128,2048]{1,0:T(8,128)(2,1)} copy(bf16[128,2048]{1,0:T(8,128)(2,1)} %shard_map.136) | data formatting | bytes 1048576
